TPU v7x, 512 devices: a whole 4x4x16 slice. The times are simulated.
512 devices in a mesh: gr: 2 (over z_hi), sp: 32 (over z_lo, y), tp: 8 (over x, core).
Axes of the slice: x: 4, y: 4, z: 16 (z_hi: 2, z_lo: 8; z = z_hi * 8 + z_lo), core: 2. Of those that a mesh axis runs over, the one named last changes fastest.
Arguments:
- tokens: bfloat16 [8, 4096, 4096], P('gr', 'sp'), parts along dimension 0, may hold values from -6 to 6
- key_weight: bfloat16 [4096, 2048], P('sp', 'tp'), may hold values from -0.09375 to 0.09375
- value_weight: bfloat16 [4096, 2048], P('sp', 'tp'), may hold values from -0.09375 to 0.09375
- log_decay: float32 [32, 8, 4096], P('tp', 'gr', 'sp'), parts along dimension 1, may hold values from -1 to 0, as said below
- new_query: bfloat16 [8, 2048], P('gr', 'tp'), parts along dimension 0, may hold values from -6 to 6
- new_key: bfloat16 [8, 2048], P('gr', 'tp'), parts along dimension 0, may hold values from -24 to 24
- new_value: bfloat16 [8, 2048], P('gr', 'tp'), parts along dimension 0, may hold values from -6 to 6
- step_decay: float32 [32, 8], P('tp', 'gr'), parts along dimension 1, may hold values from -1.5 to -0.05
- norm_gain: float32 [2048], P('tp'), may hold values from 0.1 to 1.9
Outputs:
- state_cache: float32 [512, 32, 64], P('gr', 'tp'), parts along dimension 0
- first_read: bfloat16 [8, 2048], P('gr', 'tp'), parts along dimension 0
There are 2 independent parts, one for each index of `gr`. A program takes and returns all parts, laid end to end along the dimension named above; an argument that names none is the same for every part. Nothing has to cross between parts.
Inputs may be any that keep to these rules, and one draw needn't show every extreme that they name: `log_decay`: every entry is at most zero.
All inputs are finite; a program needn't handle non-finite values.
Results may differ from a plain program's by a relative error of at most 0.0053.
Values may be sent and summed in bfloat16 or wider, within the bound.
No kernel may reach another device: no remote copies, remote signals or barrier semaphores. Data moves between devices by JAX's collectives and lax.ppermute only.
A program may use at most 64 MiB of HBM per device.

v0:
```python
import functools

import jax
import jax.numpy as jnp
from jax import lax
from jax.experimental import pallas as pl
from jax.experimental.pallas import tpu as pltpu
from jax.sharding import PartitionSpec as P

HEAD_DIM = 64
Y = 4
PARTS = 3
EXTRA = 128
EXACT = lax.Precision.HIGHEST
F32, BF16 = (jnp.float32, jnp.bfloat16)


def rotate_half(values, positions):
    half = values.shape[-1] // 2
    inverse = 10000.0 ** (-jnp.arange(half, dtype=jnp.float32) * (2.0 / values.shape[-1]))
    angles = positions[..., None] * inverse
    cosine = jnp.cos(angles)
    sine = jnp.sin(angles)
    first, second = (values[..., :half], values[..., half:])
    return jnp.concatenate(
        [first * cosine - second * sine, second * cosine + first * sine], axis=-1
    )


def moved_along_z(x, by):
    ring = lax.axis_size("gr") * lax.axis_size("sp") // Y
    pairs = [(z * Y + y, (z + by) % ring * Y + y) for z in range(ring) for y in range(Y)]
    return lax.ppermute(x, ("gr", "sp"), pairs)


def from_opposite_plane(x):
    ring = lax.axis_size("gr") * lax.axis_size("sp") // Y
    wide = lax.axis_size("tp")
    far = lax.axis_size("sp") // Y // 2
    pairs = []
    for z in range(ring):
        for y in range(Y):
            for t in range(wide):
                to = (z + (far if t % 2 else -far)) % ring
                pairs.append(((z * Y + y) * wide + t, (to * Y + y) * wide + t))
    return lax.ppermute(x, ("gr", "sp", "tp"), pairs)


def copies_along_y(x):
    groups = [[z * Y + y for y in range(Y)] for z in range(lax.axis_size("sp") // Y)]
    spread = jnp.broadcast_to(x[None], (Y, *x.shape))
    got = lax.all_to_all(spread, "sp", 0, 0, tiled=True, axis_index_groups=groups)
    return got.reshape(Y * got.shape[1], got.shape[2])


def projected(token_rows, own):
    planes = lax.axis_size("sp") // Y
    far = planes // 2
    mine = lax.axis_index("sp").astype(jnp.uint32) // Y
    block = copies_along_y(own)
    opposite = from_opposite_plane(own)
    depth = block.shape[0]

    def part(weights, off):
        first = (mine + (off + planes)) % planes * depth
        cols = lax.dynamic_slice_in_dim(token_rows, first, depth, 1)
        return jnp.dot(cols, weights, preferred_element_type=jnp.float32)

    total = part(block, 0)
    down = moved_along_z(block, -1)
    up = moved_along_z(block, 1)
    spread = copies_along_y(opposite)
    for hop in range(1, far):
        total += part(up, -hop) + part(down, hop)
        if hop + 1 < far:
            up, down = moved_along_z(up, 1), moved_along_z(down, -1)
        if hop == 1:
            total, spread = lax.optimization_barrier((total, spread))
            total += part(spread, far)
    return total


def in_three(x):
    parts, rest = ([], x)
    for _ in range(PARTS):
        piece = lax.reduce_precision(rest, 8, 7)
        parts.append(piece.astype(jnp.bfloat16))
        rest = rest - piece
    return parts


def lanes_of(shape):
    return lax.broadcasted_iota(jnp.int32, shape, 1)


def rows_of(shape):
    return lax.broadcasted_iota(jnp.int32, shape, 0)


def share_kernel(seqs, sums_ref, cosine_ref, sine_ref, weight_ref, carried_ref, out_ref):
    cols = out_ref.shape[0]
    heads = cols // HEAD_DIM
    span = sums_ref.shape[0] // seqs
    half = HEAD_DIM // 2
    low = lanes_of((span, cols)) % HEAD_DIM < half
    spread = (rows_of((heads, cols)) == lanes_of((heads, cols)) // HEAD_DIM).astype(F32)
    blocks = [[] for _ in range(heads)]
    for seq in range(seqs):
        here = pl.ds(seq * span, span)
        keys = sums_ref[here, :cols].astype(BF16).astype(F32)
        values = sums_ref[here, cols:].astype(BF16)
        other = jnp.where(low, pltpu.roll(keys, cols - half, 1), pltpu.roll(keys, half, 1))
        turned = keys * cosine_ref[...] + other * sine_ref[...]
        faded = turned * jnp.dot(weight_ref[here, :], spread, precision=EXACT)
        high = faded.astype(BF16)
        rest = (faded - high.astype(F32)).astype(BF16)
        product = sum(
            lax.dot_general(
                values, part, (((0,), (0,)), ((), ())), preferred_element_type=F32
            )
            for part in (high, rest)
        )
        for head in range(heads):
            cut = slice(head * HEAD_DIM, (head + 1) * HEAD_DIM)
            blocks[head].append(product[cut, cut])
    for head in range(heads):
        cut = pl.ds(head * HEAD_DIM, HEAD_DIM)
        out_ref[cut, : seqs * HEAD_DIM] = jnp.concatenate(blocks[head], axis=1).astype(BF16)
    out_ref[:, seqs * HEAD_DIM :] = carried_ref[...]


def owner_kernel(devices, seqs, got_ref, lines_ref, values_ref, out_ref):
    total, lanes = (got_ref.shape[0], seqs * HEAD_DIM)
    rows = total // devices
    later = (lanes_of((devices, total)) // rows > rows_of((devices, total))) & (
        lanes_of((devices, total)) % rows == 0
    )
    sums = jnp.dot(later.astype(BF16), got_ref[:, lanes:], preferred_element_type=F32)
    place = (EXTRA, lanes)
    wide = (rows_of(place) // PARTS == lanes_of(place) // HEAD_DIM).astype(F32)
    fade = jnp.exp(jnp.dot(sums, wide, precision=EXACT))
    shares = got_ref[:, :lanes].astype(F32)
    owned = shares[:rows] * fade[0:1]
    for device in range(1, devices):
        owned += shares[device * rows : (device + 1) * rows] * fade[device : device + 1]
    finished = lines_ref[0:1] * owned + lines_ref[1:2] * values_ref[...]
    place = (lanes, EXTRA)
    fold = rows_of(place) // HEAD_DIM == lanes_of(place) % seqs
    read = jnp.dot(finished * lines_ref[2:3], fold.astype(F32), precision=EXACT)
    piece = lanes_of(read.shape) // seqs
    rest, packed = (read, jnp.zeros_like(read))
    for part in range(PARTS):
        rounded = rest.astype(BF16).astype(F32)
        packed = jnp.where(piece == part, rounded, packed)
        rest = rest - rounded
    line = jnp.concatenate([finished, packed], axis=1)
    out_ref[...] = jnp.concatenate([line] * devices, axis=0).astype(BF16)


def read_kernel(seqs, got_ref, gain_ref, state_ref, read_ref):
    cols, lanes = (got_ref.shape[0], seqs * HEAD_DIM)
    state_ref[...] = got_ref[:, :lanes].astype(F32)
    place = (8, EXTRA)
    pick = (lanes_of(place) % seqs == rows_of(place)) & (lanes_of(place) < seqs * PARTS)
    raw = lax.dot_general(
        pick.astype(BF16), got_ref[:, lanes:], (((1,), (1,)), ((), ())), preferred_element_type=F32
    )
    place = (cols, cols)
    mean = (rows_of(place) // HEAD_DIM == lanes_of(place) // HEAD_DIM).astype(F32) / HEAD_DIM
    center = raw - jnp.dot(raw, mean, precision=EXACT)
    spread = jnp.dot(center * center, mean, precision=EXACT)
    normed = center * lax.rsqrt(spread + 1e-06) * gain_ref[...]
    read_ref[...] = normed[:seqs].astype(BF16)


def in_vmem(kernel, shapes, *operands):
    space = pl.BlockSpec(memory_space=pltpu.VMEM)
    many = isinstance(shapes, list)
    return pl.pallas_call(
        kernel,
        out_shape=shapes,
        in_specs=[space] * len(operands),
        out_specs=[space] * len(shapes) if many else space,
        compiler_params=pltpu.CompilerParams(vmem_limit_bytes=16 * 2**20),
    )(*operands)


def shards(
    tokens,
    key_weight,
    value_weight,
    log_decay,
    new_query,
    new_key,
    new_value,
    step_decay,
    norm_gain,
):
    seqs, span, width = tokens.shape
    heads = key_weight.shape[1] // HEAD_DIM
    cols = heads * HEAD_DIM
    lanes = seqs * HEAD_DIM
    half = HEAD_DIM // 2
    devices, mine = (lax.axis_size("sp"), lax.axis_index("sp"))
    rows = cols // devices

    positions = (mine * span + jnp.arange(span, dtype=jnp.int32)).astype(F32)
    inverse = 10000.0 ** (-jnp.arange(half, dtype=F32) * (2.0 / HEAD_DIM))
    angles = positions[:, None] * inverse
    cosine = jnp.tile(jnp.cos(angles), (1, 2 * heads)) * HEAD_DIM ** (-0.5)
    sine = jnp.sin(angles) * HEAD_DIM ** (-0.5)
    sine = jnp.tile(jnp.concatenate([-sine, sine], axis=1), (1, heads))
    totals = jnp.sum(log_decay, axis=-1)
    weight = jnp.exp(totals[:, :, None] - jnp.cumsum(log_decay, axis=-1))
    weight = jnp.transpose(weight, (1, 2, 0)).reshape(seqs * span, heads)
    carried = jnp.stack(in_three(totals), axis=-1).reshape(heads, 1, 1, seqs * PARTS)
    carried = jnp.broadcast_to(carried, (heads, devices // heads, 1, seqs * PARTS))
    carried = carried.reshape(devices, 1, seqs * PARTS)
    carried = jnp.pad(carried, ((0, 0), (0, rows - 1), (0, EXTRA - seqs * PARTS)))
    carried = carried.reshape(cols, EXTRA)

    end_pos = jnp.full((seqs, heads), float(span * devices), F32)
    query = rotate_half(new_query.astype(F32).reshape(seqs, heads, HEAD_DIM), end_pos)
    key_new = rotate_half(
        new_key.astype(F32).reshape(seqs, heads, HEAD_DIM), end_pos
    ) * HEAD_DIM ** (-0.5)
    decay_lanes = jnp.repeat(jnp.exp(step_decay), HEAD_DIM, axis=1)
    by_head = [jnp.transpose(x, (1, 0, 2)).reshape(heads, lanes) for x in (key_new, query)]
    lines = jnp.stack([decay_lanes, *by_head], axis=1)
    lines = lax.dynamic_index_in_dim(lines, mine // (devices // heads), 0, keepdims=False)
    value_cols = jnp.repeat(new_value.astype(F32).T, HEAD_DIM, axis=1)
    value_rows = lax.dynamic_slice_in_dim(value_cols, mine * rows, rows, 0)
    ready = lax.optimization_barrier((cosine, sine, weight, carried, lines, value_rows))
    cosine, sine, weight, carried, lines, value_rows = ready

    own = jnp.concatenate([key_weight, value_weight], axis=1)
    sums = projected(tokens.reshape(seqs * span, width), own)
    whole = jax.ShapeDtypeStruct((cols, lanes + EXTRA), BF16)

    def exchanged(x):
        cut = x.reshape(devices, rows, lanes + EXTRA)
        return lax.all_to_all(cut, "sp", 0, 0, tiled=True).reshape(x.shape)

    sent = in_vmem(
        functools.partial(share_kernel, seqs), whole, sums, cosine, sine, weight, carried
    )
    finished = in_vmem(
        functools.partial(owner_kernel, devices, seqs), whole, exchanged(sent), lines, value_rows
    )
    state, first_read = in_vmem(
        functools.partial(read_kernel, seqs),
        [jax.ShapeDtypeStruct((cols, lanes), F32), jax.ShapeDtypeStruct((seqs, cols), BF16)],
        exchanged(finished),
        norm_gain.reshape(1, cols),
    )
    state_cache = jnp.transpose(state.reshape(heads, HEAD_DIM, lanes), (2, 0, 1))
    return (state_cache, first_read)


def solution(mesh):
    placed = (
        P("gr", "sp", None),
        P("sp", "tp"),
        P("sp", "tp"),
        P("tp", "gr", "sp"),
        P("gr", "tp"),
        P("gr", "tp"),
        P("gr", "tp"),
        P("tp", "gr"),
        P("tp"),
    )
    return jax.shard_map(
        shards,
        mesh=mesh,
        in_specs=placed,
        out_specs=(P("gr", "tp", None), P("gr", "tp")),
        check_vma=False,
    )
```

profile of v0, /device:TPU:4, one launch (start us, length us, event | category | flops | bytes accessed | tf_op | source)
XLA Modules:
  0.0 132.6 jit_solution(8928433248698950452)
XLA Ops:
  0.6 0.8 constant_dynamic-update-slice_fusion.1
  1.5 0.8 constant_dynamic-update-slice_fusion
  2.3 12.7 %collective-permute-start.2 = (bf16[128,512]{1,0:T(8,128)(2,1)S(1)}, bf16[128,512]{1,0:T(8,128)(2,1)S(1)}, u32[]{:S(2)}, u32[]{:S(2)}) collective-permute-start(bf16[128,512]{1,0:T(8,128)(2,1)S(1)} %constant_dynamic-update-slice_fusion), channel_id=1, source_target_pairs={{0,384},{1,129},{2,386},{3,131},{4,388},{5,133},{6,390},{7,135},{8... | collective-permute-start | bytes 393224 | tf_op jit(solution)/shard_map/ppermute | solution.py:46
  15.1 0.8 broadcast_in_dim.14
  15.9 4.5 %all-to-all-start = ((bf16[4,128,512]{2,1,0:T(8,128)(2,1)}), bf16[4,128,512]{2,1,0:T(8,128)(2,1)S(1)}, u32[]{:S(2)}, u32[]{:S(2)}) async-start(bf16[4,128,512]{2,1,0:T(8,128)(2,1)} %broadcast_in_dim.14), calls=%async_computation | async-start | bytes 1048576 | tf_op jit(solution)/shard_map/all_to_all | solution.py:52
  20.4 2.3 %reduce_window_sum.13 = f32[4,4,128]{2,1,0:T(4,128)S(1)} reduce-window(f32[4,4,128]{2,1,0:T(4,128)} %param.12, f32[]{:T(128)} %constant.100.clone.1), window={size=1x1x128 pad=0_0x0_0x127_0}, to_apply=%region_1.0 | reduce-window | flops 260096 | bytes 16388 | tf_op jit(solution)/shard_map/jit(cumsum)/reduce_window_sum | solution.py:214
  22.6 0.8 reduce_sum.11
  23.5 0.1 copy.17
  23.6 0.1 broadcast_in_dim.16
  23.7 0.7 convert_bitcast_fusion
  24.4 0.1 fusion.19
  24.6 0.1 fusion.18
  24.7 0.8 reshape.171
  25.5 0.8 reshape.169
  26.3 0.1 constant_dynamic-slice_fusion
  26.4 0.1 multiply_subtract_fusion
  26.5 2.0 %all-to-all-done = bf16[4,128,512]{2,1,0:T(8,128)(2,1)S(1)} async-done(((bf16[4,128,512]{2,1,0:T(8,128)(2,1)}), bf16[4,128,512]{2,1,0:T(8,128)(2,1)S(1)}, u32[]{:S(2)}, u32[]{:S(2)}) %all-to-all-start) | async-done | bytes 524320 | tf_op jit(solution)/shard_map/all_to_all | solution.py:52
  28.4 4.1 %collective-permute-start.1 = (bf16[512,512]{1,0:T(8,128)(2,1)S(1)}, bf16[512,512]{1,0:T(8,128)(2,1)S(1)}, u32[]{:S(2)}, u32[]{:S(2)}) collective-permute-start(bf16[512,512]{1,0:T(8,128)(2,1)S(1)} %bitcast.61), channel_id=1, source_target_pairs={{0,480},{8,488},{16,496},{24,504},{32,0},{40,8},{48,16},{56,24},{6... | collective-permute-start | bytes 1572872 | tf_op jit(solution)/shard_map/ppermute | solution.py:33
  32.6 0.1 fusion.17
  32.6 0.7 exp.8
  33.3 0.1 broadcast_in_dim.37
  33.4 0.1 stack_reshape.9
  33.5 0.1 stack_reshape.10
  33.6 0.1 stack_reshape.11
  33.7 0.1 copy.16
  33.9 0.1 copy.24.values_ref
  34.0 0.1 copy.22.cosine_ref
  34.1 0.1 copy.23.sine_ref
  34.2 0.0 collective-permute-done.2
  34.2 0.8 broadcast_in_dim.15
  35.0 3.5 %all-to-all-start.1 = ((bf16[4,128,512]{2,1,0:T(8,128)(2,1)}), bf16[4,128,512]{2,1,0:T(8,128)(2,1)S(1)}, u32[]{:S(2)}, u32[]{:S(2)}) async-start(bf16[4,128,512]{2,1,0:T(8,128)(2,1)} %broadcast_in_dim.15), calls=%async_computation.1 | async-start | bytes 1048576 | tf_op jit(solution)/shard_map/all_to_all | solution.py:52
  38.5 1.9 %collective-permute-start = (bf16[512,512]{1,0:T(8,128)(2,1)S(1)}, bf16[512,512]{1,0:T(8,128)(2,1)}, u32[]{:S(2)}, u32[]{:S(2)}) collective-permute-start(bf16[512,512]{1,0:T(8,128)(2,1)S(1)} %bitcast.62), channel_id=1, source_target_pairs={{0,32},{8,40},{16,48},{24,56},{32,64},{40,72},{48,80},{56,88},{64,... | collective-permute-start | bytes 1572872 | tf_op jit(solution)/shard_map/ppermute | solution.py:33
  40.5 1.5 %fusion.13 = f32[512,512]{1,0:T(8,128)S(1)} fusion(bf16[512,512]{1,0:T(8,128)(2,1)S(1)} %bitcast.63, bf16[512,4096]{1,0:T(8,128)(2,1)} %bitcast.53, u32[]{:T(128)S(6)} %mul.142), kind=kOutput, calls=%fused_computation.17 | convolution fusion | flops 268435456 | bytes 2097156 | tf_op jit(solution)/shard_map/dot_general | solution.py:67
  41.9 0.0 collective-permute-done.1
  42.0 5.1 %collective-permute-start.4 = (bf16[512,512]{1,0:T(8,128)(2,1)S(1)}, bf16[512,512]{1,0:T(8,128)(2,1)S(1)}, u32[]{:S(2)}, u32[]{:S(2)}) collective-permute-start(bf16[512,512]{1,0:T(8,128)(2,1)S(1)} %collective-permute-done.1), channel_id=1, source_target_pairs={{0,480},{8,488},{16,496},{24,504},{32,0},{40,8},{48,16},{56,24},{6... | collective-permute-start | bytes 1572872 | tf_op jit(solution)/shard_map/ppermute | solution.py:33
  47.1 1.5 %fusion.10 = f32[512,512]{1,0:T(8,128)S(1)} fusion(bf16[512,512]{1,0:T(8,128)(2,1)S(1)} %collective-permute-done.1, bf16[512,4096]{1,0:T(8,128)(2,1)} %bitcast.54, u32[]{:T(128)S(6)} %mul.144), kind=kOutput, calls=%fused_computation.14 | convolution fusion | flops 268435456 | bytes 2097156 | tf_op jit(solution)/shard_map/dot_general | solution.py:67
  48.6 2.7 %collective-permute-done = bf16[512,512]{1,0:T(8,128)(2,1)} collective-permute-done((bf16[512,512]{1,0:T(8,128)(2,1)S(1)}, bf16[512,512]{1,0:T(8,128)(2,1)}, u32[]{:S(2)}, u32[]{:S(2)}) %collective-permute-start) | collective-permute-done | bytes 524320 | tf_op jit(solution)/shard_map/ppermute | solution.py:33
  51.3 1.9 %collective-permute-start.3 = (bf16[512,512]{1,0:T(8,128)(2,1)}, bf16[512,512]{1,0:T(8,128)(2,1)}, u32[]{:S(2)}, u32[]{:S(2)}) collective-permute-start(bf16[512,512]{1,0:T(8,128)(2,1)} %collective-permute-done), channel_id=1, source_target_pairs={{0,32},{8,40},{16,48},{24,56},{32,64},{40,72},{48,80},{56,88},{64,... | collective-permute-start | bytes 1572872 | tf_op jit(solution)/shard_map/ppermute | solution.py:33
  53.2 1.6 %fusion.2 = f32[512,512]{1,0:T(8,128)S(1)} fusion(f32[512,512]{1,0:T(8,128)S(1)} %fusion.13, f32[512,512]{1,0:T(8,128)S(1)} %fusion.10, bf16[512,512]{1,0:T(8,128)(2,1)} %collective-permute-done, bf16[512,4096]{1,0:T(8,128)(2,1)} %bitcast.55, u32[]{:T(128)S(6)} %mul.143), kind=kOutput, calls=%fused_computation.6 | convolution fusion | flops 268959744 | bytes 4194308 | tf_op jit(solution)/shard_map/dot_general | solution.py:67
  54.9 0.0 all-to-all-done.1
  54.9 1.5 %convolution_add_fusion.2 = f32[512,512]{1,0:T(8,128)S(1)} fusion(f32[512,512]{1,0:T(8,128)S(1)} %fusion.2, bf16[512,512]{1,0:T(8,128)(2,1)S(1)} %bitcast.64, bf16[512,4096]{1,0:T(8,128)(2,1)} %bitcast.56, u32[]{:T(128)S(6)} %mul.145), kind=kOutput, calls=%fused_computation.4 | convolution fusion | flops 268697600 | bytes 3145732 | tf_op jit(solution)/shard_map/dot_general | solution.py:67
  56.4 0.0 collective-permute-done.4
  56.4 5.1 %collective-permute-start.6 = (bf16[512,512]{1,0:T(8,128)(2,1)S(1)}, bf16[512,512]{1,0:T(8,128)(2,1)S(1)}, u32[]{:S(2)}, u32[]{:S(2)}) collective-permute-start(bf16[512,512]{1,0:T(8,128)(2,1)S(1)} %collective-permute-done.4), channel_id=1, source_target_pairs={{0,480},{8,488},{16,496},{24,504},{32,0},{40,8},{48,16},{56,24},{6... | collective-permute-start | bytes 1572872 | tf_op jit(solution)/shard_map/ppermute | solution.py:33
  61.5 3.9 %collective-permute-done.3 = bf16[512,512]{1,0:T(8,128)(2,1)} collective-permute-done((bf16[512,512]{1,0:T(8,128)(2,1)}, bf16[512,512]{1,0:T(8,128)(2,1)}, u32[]{:S(2)}, u32[]{:S(2)}) %collective-permute-start.3) | collective-permute-done | bytes 524320 | tf_op jit(solution)/shard_map/ppermute | solution.py:33
  65.4 1.9 %collective-permute-start.5 = (bf16[512,512]{1,0:T(8,128)(2,1)}, bf16[512,512]{1,0:T(8,128)(2,1)S(1)}, u32[]{:S(2)}, u32[]{:S(2)}) collective-permute-start(bf16[512,512]{1,0:T(8,128)(2,1)} %collective-permute-done.3), channel_id=1, source_target_pairs={{0,32},{8,40},{16,48},{24,56},{32,64},{40,72},{48,80},{56,88},{64,... | collective-permute-start | bytes 1572872 | tf_op jit(solution)/shard_map/ppermute | solution.py:33
  67.3 1.5 %fusion.6 = f32[512,512]{1,0:T(8,128)S(1)} fusion(bf16[512,512]{1,0:T(8,128)(2,1)S(1)} %collective-permute-done.4, bf16[512,4096]{1,0:T(8,128)(2,1)} %bitcast.57, u32[]{:T(128)S(6)} %mul.147), kind=kOutput, calls=%fused_computation.10 | convolution fusion | flops 268435456 | bytes 2097156 | tf_op jit(solution)/shard_map/dot_general | solution.py:67
  68.8 1.6 %fusion.1 = f32[512,512]{1,0:T(8,128)S(1)} fusion(f32[512,512]{1,0:T(8,128)S(1)} %convolution_add_fusion.2, f32[512,512]{1,0:T(8,128)S(1)} %fusion.6, bf16[512,512]{1,0:T(8,128)(2,1)} %collective-permute-done.3, bf16[512,4096]{1,0:T(8,128)(2,1)} %bitcast.58, u32[]{:T(128)S(6)} %mul.146), kind=kOutput, calls=%fused_computation.3 | convolution fusion | flops 268959744 | bytes 4194308 | tf_op jit(solution)/shard_map/dot_general | solution.py:67
  70.4 0.0 copy-start
  70.5 0.0 collective-permute-done.6
  70.5 1.5 %fusion.3 = f32[512,512]{1,0:T(8,128)S(1)} fusion(bf16[512,512]{1,0:T(8,128)(2,1)S(1)} %collective-permute-done.6, bf16[512,4096]{1,0:T(8,128)(2,1)} %bitcast.59, u32[]{:T(128)S(6)} %mul.149), kind=kOutput, calls=%fused_computation.7 | convolution fusion | flops 268435456 | bytes 2097156 | tf_op jit(solution)/shard_map/dot_general | solution.py:67
  72.0 5.9 %collective-permute-done.5 = bf16[512,512]{1,0:T(8,128)(2,1)S(1)} collective-permute-done((bf16[512,512]{1,0:T(8,128)(2,1)}, bf16[512,512]{1,0:T(8,128)(2,1)S(1)}, u32[]{:S(2)}, u32[]{:S(2)}) %collective-permute-start.5) | collective-permute-done | bytes 524320 | tf_op jit(solution)/shard_map/ppermute | solution.py:33
  77.9 1.5 %fusion.sums_ref = f32[512,512]{1,0:T(8,128)S(1)} fusion(f32[512,512]{1,0:T(8,128)S(1)} %fusion.1, f32[512,512]{1,0:T(8,128)S(1)} %fusion.3, bf16[512,512]{1,0:T(8,128)(2,1)S(1)} %collective-permute-done.5, bf16[512,4096]{1,0:T(8,128)(2,1)} %bitcast.60, u32[]{:T(128)S(6)} %mul.148), kind=kOutput, calls=%fused_computation.1 | convolution fusion | flops 268959744 | bytes 4194308 | tf_op jit(solution)/shard_map/dot_general | solution.py:67
  79.4 2.0 %shard_map.104 = bf16[256,384]{1,0:T(8,128)(2,1)S(1)} custom-call(f32[512,512]{1,0:T(8,128)S(1)} %fusion.sums_ref, f32[128,256]{1,0:T(8,128)S(1)} %copy.22.cosine_ref, f32[128,256]{1,0:T(8,128)S(1)} %copy.23.sine_ref, f32[512,4]{1,0:T(8,128)S(1)} %bitcast.47, bf16[256,128]{1,0:T(8,128)(2,1)S(1)} %pad_bitcast_fusion.carried_ref), custom_call_target="tpu_custom_call" | custom-call | tf_op jit(solution)/shard_map/pallas_call | solution.py:179
  81.4 28.3 %all_to_all.20 = bf16[32,8,384]{2,1,0:T(8,128)(2,1)S(1)} all-to-all(bf16[32,8,384]{2,1,0:T(8,128)(2,1)S(1)} %bitcast.48), channel_id=1, replica_groups=mesh['gr'=2,'sp'=32,'tp'=8] {'sp'}, dimensions={0} | all-to-all | bytes 393216 | tf_op jit(solution)/shard_map/all_to_all | solution.py:242
  109.7 0.6 shard_map.105
  110.3 21.1 %all_to_all.21 = bf16[32,8,384]{2,1,0:T(8,128)(2,1)S(1)} all-to-all(bf16[32,8,384]{2,1,0:T(8,128)(2,1)S(1)} %bitcast.50), channel_id=1, replica_groups=mesh['gr'=2,'sp'=32,'tp'=8] {'sp'}, dimensions={0} | all-to-all | bytes 393216 | tf_op jit(solution)/shard_map/all_to_all | solution.py:242
  131.3 0.0 copy-done
  131.3 1.3 shard_map.106
  (16 shorter events, 0.2 us)
Async XLA Ops:
  2.3 31.9 %collective-permute-start.2 = (bf16[128,512]{1,0:T(8,128)(2,1)S(1)}, bf16[128,512]{1,0:T(8,128)(2,1)S(1)}, u32[]{:S(2)}, u32[]{:S(2)}) collective-permute-start(bf16[128,512]{1,0:T(8,128)(2,1)S(1)} %constant_dynamic-update-slice_fusion), channel_id=1, source_target_pairs={{0,384},{1,129},{2,386},{3,131},{4,388},{5,133},{6,390},{7,135},{8... | collective-permute-start | bytes 393224 | tf_op jit(solution)/shard_map/ppermute | solution.py:46
  15.9 12.5 %all-to-all-start = ((bf16[4,128,512]{2,1,0:T(8,128)(2,1)}), bf16[4,128,512]{2,1,0:T(8,128)(2,1)S(1)}, u32[]{:S(2)}, u32[]{:S(2)}) async-start(bf16[4,128,512]{2,1,0:T(8,128)(2,1)} %broadcast_in_dim.14), calls=%async_computation | async-start | bytes 1048576 | tf_op jit(solution)/shard_map/all_to_all | solution.py:52
  28.4 13.5 %collective-permute-start.1 = (bf16[512,512]{1,0:T(8,128)(2,1)S(1)}, bf16[512,512]{1,0:T(8,128)(2,1)S(1)}, u32[]{:S(2)}, u32[]{:S(2)}) collective-permute-start(bf16[512,512]{1,0:T(8,128)(2,1)S(1)} %bitcast.61), channel_id=1, source_target_pairs={{0,480},{8,488},{16,496},{24,504},{32,0},{40,8},{48,16},{56,24},{6... | collective-permute-start | bytes 1572872 | tf_op jit(solution)/shard_map/ppermute | solution.py:33
  35.0 19.8 %all-to-all-start.1 = ((bf16[4,128,512]{2,1,0:T(8,128)(2,1)}), bf16[4,128,512]{2,1,0:T(8,128)(2,1)S(1)}, u32[]{:S(2)}, u32[]{:S(2)}) async-start(bf16[4,128,512]{2,1,0:T(8,128)(2,1)} %broadcast_in_dim.15), calls=%async_computation.1 | async-start | bytes 1048576 | tf_op jit(solution)/shard_map/all_to_all | solution.py:52
  38.5 12.8 %collective-permute-start = (bf16[512,512]{1,0:T(8,128)(2,1)S(1)}, bf16[512,512]{1,0:T(8,128)(2,1)}, u32[]{:S(2)}, u32[]{:S(2)}) collective-permute-start(bf16[512,512]{1,0:T(8,128)(2,1)S(1)} %bitcast.62), channel_id=1, source_target_pairs={{0,32},{8,40},{16,48},{24,56},{32,64},{40,72},{48,80},{56,88},{64,... | collective-permute-start | bytes 1572872 | tf_op jit(solution)/shard_map/ppermute | solution.py:33
  42.0 14.4 %collective-permute-start.4 = (bf16[512,512]{1,0:T(8,128)(2,1)S(1)}, bf16[512,512]{1,0:T(8,128)(2,1)S(1)}, u32[]{:S(2)}, u32[]{:S(2)}) collective-permute-start(bf16[512,512]{1,0:T(8,128)(2,1)S(1)} %collective-permute-done.1), channel_id=1, source_target_pairs={{0,480},{8,488},{16,496},{24,504},{32,0},{40,8},{48,16},{56,24},{6... | collective-permute-start | bytes 1572872 | tf_op jit(solution)/shard_map/ppermute | solution.py:33
  51.3 14.1 %collective-permute-start.3 = (bf16[512,512]{1,0:T(8,128)(2,1)}, bf16[512,512]{1,0:T(8,128)(2,1)}, u32[]{:S(2)}, u32[]{:S(2)}) collective-permute-start(bf16[512,512]{1,0:T(8,128)(2,1)} %collective-permute-done), channel_id=1, source_target_pairs={{0,32},{8,40},{16,48},{24,56},{32,64},{40,72},{48,80},{56,88},{64,... | collective-permute-start | bytes 1572872 | tf_op jit(solution)/shard_map/ppermute | solution.py:33
  56.4 14.1 %collective-permute-start.6 = (bf16[512,512]{1,0:T(8,128)(2,1)S(1)}, bf16[512,512]{1,0:T(8,128)(2,1)S(1)}, u32[]{:S(2)}, u32[]{:S(2)}) collective-permute-start(bf16[512,512]{1,0:T(8,128)(2,1)S(1)} %collective-permute-done.4), channel_id=1, source_target_pairs={{0,480},{8,488},{16,496},{24,504},{32,0},{40,8},{48,16},{56,24},{6... | collective-permute-start | bytes 1572872 | tf_op jit(solution)/shard_map/ppermute | solution.py:33
  65.4 12.5 %collective-permute-start.5 = (bf16[512,512]{1,0:T(8,128)(2,1)}, bf16[512,512]{1,0:T(8,128)(2,1)S(1)}, u32[]{:S(2)}, u32[]{:S(2)}) collective-permute-start(bf16[512,512]{1,0:T(8,128)(2,1)} %collective-permute-done.3), channel_id=1, source_target_pairs={{0,32},{8,40},{16,48},{24,56},{32,64},{40,72},{48,80},{56,88},{64,... | collective-permute-start | bytes 1572872 | tf_op jit(solution)/shard_map/ppermute | solution.py:33
  70.4 60.9 %copy-start = (f32[256]{0:T(256)S(1)}, f32[256]{0:T(256)}, u32[]{:S(2)}) copy-start(f32[256]{0:T(256)} %param.17) | copy-start | bytes 3076
where the time goes:
time: 134 us; the launch traced here: 133 us
  blocking collectives  49.3 us (37%)
  starting transfers between devices  40.8 us (30%)
  waiting for transfers between devices  14.5 us (11%)
  matrix products  12.2 us (9%)
  local copies, waits for them, and re-layouts  6.71 us (5%)
  other arithmetic  4.26 us (3%)
  Pallas kernels  3.94 us (3%)
    all_to_all x2, blocking collectives, exchanged(): return lax.all_to_all(cut, 'sp', 0, 0, tiled=True).reshape(x.shape)  49.3 us
    ppermute x6, starting transfers between devices, moved_along_z(): return lax.ppermute(x, ('gr', 'sp'), pairs)  20.1 us
    ppermute x1, starting transfers between devices, from_opposite_plane(): return lax.ppermute(x, ('gr', 'sp', 'tp'), pairs)  12.7 us
    ppermute x6, waiting for transfers between devices, moved_along_z(): return lax.ppermute(x, ('gr', 'sp'), pairs)  12.5 us
    dot_general x8, matrix products, part(): return jnp.dot(cols, weights, preferred_element_type=jnp.float32)  12.2 us
    all_to_all x2, starting transfers between devices, copies_along_y(): lax.all_to_all(spread, 'sp', 0, 0, tiled=True, axis_index_groups=groups)  7.93 us
    pallas_call x3, Pallas kernels, in_vmem(): pl.pallas_call(kernel, out_shape=shapes, in_specs=[space] * len(operands)...  3.94 us
  transfers between devices with their start and end apart: 9, of which 4 were waited for; matrix products, arithmetic and copies ran while one was open for 15% of the time, Pallas kernels for 0%

commit v1 on v0

--- a/solution.py
+++ b/solution.py
@@ -46,38 +46,35 @@
     return lax.ppermute(x, ("gr", "sp", "tp"), pairs)
 
 
-def copies_along_y(x):
+def exchanged_along_y(spread):
     groups = [[z * Y + y for y in range(Y)] for z in range(lax.axis_size("sp") // Y)]
-    spread = jnp.broadcast_to(x[None], (Y, *x.shape))
     got = lax.all_to_all(spread, "sp", 0, 0, tiled=True, axis_index_groups=groups)
     return got.reshape(Y * got.shape[1], got.shape[2])
 
 
-def projected(token_rows, own):
+def projected(token_rows, own, spread):
     planes = lax.axis_size("sp") // Y
     far = planes // 2
     mine = lax.axis_index("sp").astype(jnp.uint32) // Y
-    block = copies_along_y(own)
+    block = exchanged_along_y(spread)
     opposite = from_opposite_plane(own)
     depth = block.shape[0]
 
     def part(weights, off):
         first = (mine + (off + planes)) % planes * depth
         cols = lax.dynamic_slice_in_dim(token_rows, first, depth, 1)
-        return jnp.dot(cols, weights, preferred_element_type=jnp.float32)
+        return jnp.dot(cols, weights, preferred_element_type=F32)
 
     total = part(block, 0)
-    down = moved_along_z(block, -1)
-    up = moved_along_z(block, 1)
-    spread = copies_along_y(opposite)
+    up = down = block
     for hop in range(1, far):
-        total += part(up, -hop) + part(down, hop)
+        down = moved_along_z(down, -1)
+        up = moved_along_z(up, 1)
         if hop + 1 < far:
-            up, down = moved_along_z(up, 1), moved_along_z(down, -1)
-        if hop == 1:
-            total, spread = lax.optimization_barrier((total, spread))
-            total += part(spread, far)
-    return total
+            total += part(up, -hop) + part(down, hop)
+    distant = exchanged_along_y(jnp.broadcast_to(opposite[None], (Y, *opposite.shape)))
+    total += part(distant, far)
+    return total + part(up, 1 - far) + part(down, far - 1)
 
 
 def in_three(x):
@@ -95,6 +92,13 @@
 
 def rows_of(shape):
     return lax.broadcasted_iota(jnp.int32, shape, 0)
+
+
+def spread_kernel(key_ref, value_ref, own_ref, spread_ref):
+    both = jnp.concatenate([key_ref[...], value_ref[...]], axis=1)
+    own_ref[...] = both
+    for y in range(Y):
+        spread_ref[y] = both
 
 
 def share_kernel(seqs, sums_ref, cosine_ref, sine_ref, weight_ref, carried_ref, out_ref):
@@ -230,11 +234,20 @@
     lines = lax.dynamic_index_in_dim(lines, mine // (devices // heads), 0, keepdims=False)
     value_cols = jnp.repeat(new_value.astype(F32).T, HEAD_DIM, axis=1)
     value_rows = lax.dynamic_slice_in_dim(value_cols, mine * rows, rows, 0)
-    ready = lax.optimization_barrier((cosine, sine, weight, carried, lines, value_rows))
-    cosine, sine, weight, carried, lines, value_rows = ready
-
-    own = jnp.concatenate([key_weight, value_weight], axis=1)
-    sums = projected(tokens.reshape(seqs * span, width), own)
+    ready = lax.optimization_barrier((cosine, sine, weight, carried))
+    cosine, sine, weight, carried = ready
+
+    depth = key_weight.shape[0]
+    own, spread = in_vmem(
+        spread_kernel,
+        [
+            jax.ShapeDtypeStruct((depth, 2 * cols), BF16),
+            jax.ShapeDtypeStruct((Y, depth, 2 * cols), BF16),
+        ],
+        key_weight,
+        value_weight,
+    )
+    sums = projected(tokens.reshape(seqs * span, width), own, spread)
     whole = jax.ShapeDtypeStruct((cols, lanes + EXTRA), BF16)
 
     def exchanged(x):

time: 134 us -> 130 us (0.970)
  blocking collectives: 49.3 us -> 21.2 us
  starting transfers between devices: 40.8 us -> 53.3 us
  waiting for transfers between devices: 14.5 us -> 26.6 us
  Pallas kernels: 3.94 us -> 5.46 us
  local copies, waits for them, and re-layouts: 6.71 us -> 5.21 us
    all_to_all x2 -> x1, blocking collectives: 49.3 us -> 21.2 us  [exchanged(): return lax.all_to_all(cut, 'sp', 0, 0, tiled=True).reshape(x.shape)]
    all_to_all x2 -> x3, waiting for transfers between devices: 1.98 us -> 14.9 us  [the longest x1 14.9 us: exchanged(): return lax.all_to_all(cut, 'sp', 0, 0, tiled=True).reshape(x.shape)]
    all_to_all x2 -> x3, starting transfers between devices: 7.93 us -> 19.5 us  [the longest x1 10.7 us: exchanged(): return lax.all_to_all(cut, 'sp', 0, 0, tiled=True).reshape(x.shape)]
    pallas_call x3 -> x4, Pallas kernels: 3.94 us -> 5.46 us  [in_vmem(): pl.pallas_call(kernel, out_shape=shapes, in_specs=[space] * len(operands)...]
  transfers between devices with their start and end apart: 9 -> 10, of which waited for: 4 -> 4; matrix products, arithmetic and copies ran while one was open for 15% -> 14% of each run, Pallas kernels for 0% -> 0%
where the time goes in v1:
time: 130 us; the launch traced here: 129 us
  starting transfers between devices  53.3 us (41%)
  waiting for transfers between devices  26.6 us (20%)
  blocking collectives  21.2 us (16%)
  matrix products  12.2 us (9%)
  Pallas kernels  5.46 us (4%)
  local copies, waits for them, and re-layouts  5.21 us (4%)
  other arithmetic  3.58 us (3%)
    all_to_all x1, blocking collectives, exchanged(): return lax.all_to_all(cut, 'sp', 0, 0, tiled=True).reshape(x.shape)  21.2 us
    ppermute x6, starting transfers between devices, moved_along_z(): return lax.ppermute(x, ('gr', 'sp'), pairs)  21 us
    all_to_all x1, waiting for transfers between devices, exchanged(): return lax.all_to_all(cut, 'sp', 0, 0, tiled=True).reshape(x.shape)  14.9 us
    ppermute x1, starting transfers between devices, from_opposite_plane(): return lax.ppermute(x, ('gr', 'sp', 'tp'), pairs)  12.7 us
    dot_general x8, matrix products, part(): return jnp.dot(cols, weights, preferred_element_type=F32)  12.2 us
    ppermute x6, waiting for transfers between devices, moved_along_z(): return lax.ppermute(x, ('gr', 'sp'), pairs)  11.7 us
    all_to_all x1, starting transfers between devices, exchanged(): return lax.all_to_all(cut, 'sp', 0, 0, tiled=True).reshape(x.shape)  10.7 us
    all_to_all x2, starting transfers between devices, exchanged_along_y(): lax.all_to_all(spread, 'sp', 0, 0, tiled=True, axis_index_groups=groups)  8.85 us
  transfers between devices with their start and end apart: 10, of which 4 were waited for; matrix products, arithmetic and copies ran while one was open for 14% of the time, Pallas kernels for 0%

profile of v1, /device:TPU:4, one launch (start us, length us, event | category | flops | bytes accessed | tf_op | source)
XLA Modules:
  0.0 128.5 jit_solution(12595368927359123458)
XLA Ops:
  0.6 0.0 copy-start
  0.6 0.8 copy-done
  1.5 0.0 copy-start.1
  1.5 0.8 copy-done.1
  2.3 0.8 shard_map.104
  3.2 4.5 %all-to-all-start = ((bf16[4,128,512]{2,1,0:T(8,128)(2,1)}), bf16[4,128,512]{2,1,0:T(8,128)(2,1)S(1)}, u32[]{:S(2)}, u32[]{:S(2)}) async-start(bf16[4,128,512]{2,1,0:T(8,128)(2,1)} %get-tuple-element.10), calls=%async_computation | async-start | bytes 1048576 | tf_op jit(solution)/shard_map/all_to_all | solution.py:51
  7.6 12.7 %collective-permute-start.4 = (bf16[128,512]{1,0:T(8,128)(2,1)S(1)}, bf16[128,512]{1,0:T(8,128)(2,1)S(1)}, u32[]{:S(2)}, u32[]{:S(2)}) collective-permute-start(bf16[128,512]{1,0:T(8,128)(2,1)S(1)} %get-tuple-element.11), channel_id=1, source_target_pairs={{0,384},{1,129},{2,386},{3,131},{4,388},{5,133},{6,390},{7,135},{8... | collective-permute-start | bytes 393224 | tf_op jit(solution)/shard_map/ppermute | solution.py:46
  20.4 0.8 reduce_sum.11
  21.2 2.3 %reduce_window_sum.13 = f32[4,4,128]{2,1,0:T(4,128)S(1)} reduce-window(f32[4,4,128]{2,1,0:T(4,128)} %param.12, f32[]{:T(128)} %constant.100.clone.1), window={size=1x1x128 pad=0_0x0_0x127_0}, to_apply=%region_1.0 | reduce-window | flops 260096 | bytes 16388 | tf_op jit(solution)/shard_map/jit(cumsum)/reduce_window_sum | solution.py:218
  23.4 0.1 copy.17
  23.6 0.1 broadcast_in_dim.13
  23.7 0.1 fusion.18
  23.8 0.1 fusion.19
  23.9 0.0 all-to-all-done
  24.0 4.5 %collective-permute-start.1 = (bf16[512,512]{1,0:T(8,128)(2,1)S(1)}, bf16[512,512]{1,0:T(8,128)(2,1)S(1)}, u32[]{:S(2)}, u32[]{:S(2)}) collective-permute-start(bf16[512,512]{1,0:T(8,128)(2,1)S(1)} %bitcast.60), channel_id=1, source_target_pairs={{0,480},{8,488},{16,496},{24,504},{32,0},{40,8},{48,16},{56,24},{6... | collective-permute-start | bytes 1572872 | tf_op jit(solution)/shard_map/ppermute | solution.py:33
  28.5 1.9 %collective-permute-start = (bf16[512,512]{1,0:T(8,128)(2,1)S(1)}, bf16[512,512]{1,0:T(8,128)(2,1)S(1)}, u32[]{:S(2)}, u32[]{:S(2)}) collective-permute-start(bf16[512,512]{1,0:T(8,128)(2,1)S(1)} %bitcast.61), channel_id=1, source_target_pairs={{0,32},{8,40},{16,48},{24,56},{32,64},{40,72},{48,80},{56,88},{64,... | collective-permute-start | bytes 1572872 | tf_op jit(solution)/shard_map/ppermute | solution.py:33
  30.5 0.1 copy.16
  30.7 0.1 copy.19.cosine_ref
  30.8 0.1 copy.20.sine_ref
  30.9 0.8 reshape.168
  31.7 0.8 reshape.170
  32.5 0.0 collective-permute-done.4
  32.5 0.8 broadcast_in_dim.12
  33.4 4.4 %all-to-all-start.1 = ((bf16[4,128,512]{2,1,0:T(8,128)(2,1)}), bf16[4,128,512]{2,1,0:T(8,128)(2,1)S(1)}, u32[]{:S(2)}, u32[]{:S(2)}) async-start(bf16[4,128,512]{2,1,0:T(8,128)(2,1)} %broadcast_in_dim.12), calls=%async_computation.1 | async-start | bytes 1048576 | tf_op jit(solution)/shard_map/all_to_all | solution.py:51
  37.8 1.5 %fusion.13 = f32[512,512]{1,0:T(8,128)S(1)} fusion(bf16[512,512]{1,0:T(8,128)(2,1)S(1)} %bitcast.62, bf16[512,4096]{1,0:T(8,128)(2,1)} %bitcast.52, u32[]{:T(128)S(6)} %mul.142), kind=kOutput, calls=%fused_computation.17 | convolution fusion | flops 268435456 | bytes 2097156 | tf_op jit(solution)/shard_map/dot_general | solution.py:66
  39.2 0.0 collective-permute-done.1
  39.2 5.1 %collective-permute-start.3 = (bf16[512,512]{1,0:T(8,128)(2,1)S(1)}, bf16[512,512]{1,0:T(8,128)(2,1)S(1)}, u32[]{:S(2)}, u32[]{:S(2)}) collective-permute-start(bf16[512,512]{1,0:T(8,128)(2,1)S(1)} %collective-permute-done.1), channel_id=1, source_target_pairs={{0,480},{8,488},{16,496},{24,504},{32,0},{40,8},{48,16},{56,24},{6... | collective-permute-start | bytes 1572872 | tf_op jit(solution)/shard_map/ppermute | solution.py:33
  44.4 0.0 collective-permute-done
  44.4 1.9 %collective-permute-start.2 = (bf16[512,512]{1,0:T(8,128)(2,1)S(1)}, bf16[512,512]{1,0:T(8,128)(2,1)}, u32[]{:S(2)}, u32[]{:S(2)}) collective-permute-start(bf16[512,512]{1,0:T(8,128)(2,1)S(1)} %collective-permute-done), channel_id=1, source_target_pairs={{0,32},{8,40},{16,48},{24,56},{32,64},{40,72},{48,80},{56,88},{64,... | collective-permute-start | bytes 1572872 | tf_op jit(solution)/shard_map/ppermute | solution.py:33
  46.3 1.5 %fusion.10 = f32[512,512]{1,0:T(8,128)S(1)} fusion(bf16[512,512]{1,0:T(8,128)(2,1)S(1)} %collective-permute-done.1, bf16[512,4096]{1,0:T(8,128)(2,1)} %bitcast.53, u32[]{:T(128)S(6)} %mul.144), kind=kOutput, calls=%fused_computation.14 | convolution fusion | flops 268435456 | bytes 2097156 | tf_op jit(solution)/shard_map/dot_general | solution.py:66
  47.8 1.5 %fusion.2 = f32[512,512]{1,0:T(8,128)S(1)} fusion(f32[512,512]{1,0:T(8,128)S(1)} %fusion.13, f32[512,512]{1,0:T(8,128)S(1)} %fusion.10, bf16[512,512]{1,0:T(8,128)(2,1)S(1)} %collective-permute-done, bf16[512,4096]{1,0:T(8,128)(2,1)} %bitcast.54, u32[]{:T(128)S(6)} %mul.143), kind=kOutput, calls=%fused_computation.6 | convolution fusion | flops 268959744 | bytes 4194308 | tf_op jit(solution)/shard_map/dot_general | solution.py:66
  49.3 4.1 %collective-permute-done.3 = bf16[512,512]{1,0:T(8,128)(2,1)S(1)} collective-permute-done((bf16[512,512]{1,0:T(8,128)(2,1)S(1)}, bf16[512,512]{1,0:T(8,128)(2,1)S(1)}, u32[]{:S(2)}, u32[]{:S(2)}) %collective-permute-start.3) | collective-permute-done | bytes 524320 | tf_op jit(solution)/shard_map/ppermute | solution.py:33
  53.4 5.6 %collective-permute-start.6 = (bf16[512,512]{1,0:T(8,128)(2,1)S(1)}, bf16[512,512]{1,0:T(8,128)(2,1)S(1)}, u32[]{:S(2)}, u32[]{:S(2)}) collective-permute-start(bf16[512,512]{1,0:T(8,128)(2,1)S(1)} %collective-permute-done.3), channel_id=1, source_target_pairs={{0,480},{8,488},{16,496},{24,504},{32,0},{40,8},{48,16},{56,24},{6... | collective-permute-start | bytes 1572872 | tf_op jit(solution)/shard_map/ppermute | solution.py:33
  59.0 1.5 %fusion.7 = f32[512,512]{1,0:T(8,128)S(1)} fusion(bf16[512,512]{1,0:T(8,128)(2,1)S(1)} %collective-permute-done.3, bf16[512,4096]{1,0:T(8,128)(2,1)} %bitcast.55, u32[]{:T(128)S(6)} %mul.146), kind=kOutput, calls=%fused_computation.11 | convolution fusion | flops 268435456 | bytes 2097156 | tf_op jit(solution)/shard_map/dot_general | solution.py:66
  60.5 0.0 collective-permute-done.2
  60.5 1.9 %collective-permute-start.5 = (bf16[512,512]{1,0:T(8,128)(2,1)}, bf16[512,512]{1,0:T(8,128)(2,1)}, u32[]{:S(2)}, u32[]{:S(2)}) collective-permute-start(bf16[512,512]{1,0:T(8,128)(2,1)} %collective-permute-done.2), channel_id=1, source_target_pairs={{0,32},{8,40},{16,48},{24,56},{32,64},{40,72},{48,80},{56,88},{64,... | collective-permute-start | bytes 1572872 | tf_op jit(solution)/shard_map/ppermute | solution.py:33
  62.4 1.6 %fusion.1 = f32[512,512]{1,0:T(8,128)S(1)} fusion(f32[512,512]{1,0:T(8,128)S(1)} %fusion.2, f32[512,512]{1,0:T(8,128)S(1)} %fusion.7, bf16[512,512]{1,0:T(8,128)(2,1)} %collective-permute-done.2, bf16[512,4096]{1,0:T(8,128)(2,1)} %bitcast.56, u32[]{:T(128)S(6)} %mul.145), kind=kOutput, calls=%fused_computation.4 | convolution fusion | flops 268959744 | bytes 4194308 | tf_op jit(solution)/shard_map/dot_general | solution.py:66
  64.1 0.0 all-to-all-done.1
  64.1 1.5 %convolution_add_fusion.1 = f32[512,512]{1,0:T(8,128)S(1)} fusion(f32[512,512]{1,0:T(8,128)S(1)} %fusion.1, bf16[512,512]{1,0:T(8,128)(2,1)S(1)} %bitcast.63, bf16[512,4096]{1,0:T(8,128)(2,1)} %bitcast.57, u32[]{:T(128)S(6)} %mul.147), kind=kOutput, calls=%fused_computation.2 | convolution fusion | flops 268697600 | bytes 3145732 | tf_op jit(solution)/shard_map/dot_general | solution.py:66
  65.6 0.0 copy-start.4
  65.6 0.0 copy-start.3
  65.6 1.9 %collective-permute-done.6 = bf16[512,512]{1,0:T(8,128)(2,1)S(1)} collective-permute-done((bf16[512,512]{1,0:T(8,128)(2,1)S(1)}, bf16[512,512]{1,0:T(8,128)(2,1)S(1)}, u32[]{:S(2)}, u32[]{:S(2)}) %collective-permute-start.6) | collective-permute-done | bytes 524320 | tf_op jit(solution)/shard_map/ppermute | solution.py:33
  67.5 1.5 %fusion.3 = f32[512,512]{1,0:T(8,128)S(1)} fusion(bf16[512,512]{1,0:T(8,128)(2,1)S(1)} %collective-permute-done.6, bf16[512,4096]{1,0:T(8,128)(2,1)} %bitcast.58, u32[]{:T(128)S(6)} %mul.149), kind=kOutput, calls=%fused_computation.7 | convolution fusion | flops 268435456 | bytes 2097156 | tf_op jit(solution)/shard_map/dot_general | solution.py:66
  69.0 0.0 copy-start.2
  69.0 5.7 %collective-permute-done.5 = bf16[512,512]{1,0:T(8,128)(2,1)} collective-permute-done((bf16[512,512]{1,0:T(8,128)(2,1)}, bf16[512,512]{1,0:T(8,128)(2,1)}, u32[]{:S(2)}, u32[]{:S(2)}) %collective-permute-start.5) | collective-permute-done | bytes 524320 | tf_op jit(solution)/shard_map/ppermute | solution.py:33
  74.7 1.6 %fusion.sums_ref = f32[512,512]{1,0:T(8,128)S(1)} fusion(f32[512,512]{1,0:T(8,128)S(1)} %fusion.3, f32[512,512]{1,0:T(8,128)S(1)} %convolution_add_fusion.1, bf16[512,512]{1,0:T(8,128)(2,1)} %collective-permute-done.5, bf16[512,4096]{1,0:T(8,128)(2,1)} %bitcast.59, u32[]{:T(128)S(6)} %mul.148), kind=kOutput, calls=%fused_computation.1 | convolution fusion | flops 268959744 | bytes 4194308 | tf_op jit(solution)/shard_map/dot_general | solution.py:66
  76.3 2.7 %shard_map.105 = bf16[256,384]{1,0:T(8,128)(2,1)} custom-call(f32[512,512]{1,0:T(8,128)S(1)} %fusion.sums_ref, f32[128,256]{1,0:T(8,128)S(1)} %copy.19.cosine_ref, f32[128,256]{1,0:T(8,128)S(1)} %copy.20.sine_ref, f32[512,4]{1,0:T(8,128)S(1)} %bitcast.47, bf16[256,128]{1,0:T(8,128)(2,1)S(1)} %pad_bitcast_fusion.carried_ref), custom_call_target="tpu_custom_call" | custom-call | tf_op jit(solution)/shard_map/pallas_call | solution.py:183
  79.0 10.7 %all-to-all-start.2 = ((bf16[32,8,384]{2,1,0:T(8,128)(2,1)}), bf16[32,8,384]{2,1,0:T(8,128)(2,1)S(1)}, u32[]{:S(2)}, u32[]{:S(2)}) async-start(bf16[32,8,384]{2,1,0:T(8,128)(2,1)} %bitcast.11), calls=%async_computation.2 | async-start | bytes 393216 | tf_op jit(solution)/shard_map/all_to_all | solution.py:255
  89.7 0.1 multiply_subtract_fusion
  89.8 0.1 fusion.17
  89.9 0.1 stack_reshape.10
  90.0 0.1 stack_reshape.11
  90.1 0.0 copy-done.4
  90.1 0.1 broadcast_in_dim.30
  90.1 0.1 stack_reshape.9
  90.2 0.0 copy-done.3
  90.3 0.1 constant_dynamic-slice_fusion
  90.4 0.1 copy.24.values_ref
  90.5 14.9 %all-to-all-done.2 = bf16[32,8,384]{2,1,0:T(8,128)(2,1)S(1)} async-done(((bf16[32,8,384]{2,1,0:T(8,128)(2,1)}), bf16[32,8,384]{2,1,0:T(8,128)(2,1)S(1)}, u32[]{:S(2)}, u32[]{:S(2)}) %all-to-all-start.2) | async-done | bytes 196640 | tf_op jit(solution)/shard_map/all_to_all | solution.py:255
  105.4 0.6 shard_map.106
  106.0 21.2 %all_to_all.20 = bf16[32,8,384]{2,1,0:T(8,128)(2,1)S(1)} all-to-all(bf16[32,8,384]{2,1,0:T(8,128)(2,1)S(1)} %bitcast.49), channel_id=1, replica_groups=mesh['gr'=2,'sp'=32,'tp'=8] {'sp'}, dimensions={0} | all-to-all | bytes 393216 | tf_op jit(solution)/shard_map/all_to_all | solution.py:255
  127.2 0.0 copy-done.2
  127.2 1.3 %shard_map.107 = (f32[256,256]{1,0:T(8,128)}, bf16[4,256]{1,0:T(4,128)(2,1)}) custom-call(bf16[256,384]{1,0:T(8,128)(2,1)S(1)} %bitcast.50, f32[1,256]{1,0:T(1,128)S(1)} %bitcast.51), custom_call_target="tpu_custom_call" | custom-call | tf_op jit(solution)/shard_map/pallas_call | solution.py:183
  (18 shorter events, 0.2 us)
Async XLA Ops:
  0.6 0.8 copy-start
  1.5 0.8 copy-start.1
  3.2 20.8 %all-to-all-start = ((bf16[4,128,512]{2,1,0:T(8,128)(2,1)}), bf16[4,128,512]{2,1,0:T(8,128)(2,1)S(1)}, u32[]{:S(2)}, u32[]{:S(2)}) async-start(bf16[4,128,512]{2,1,0:T(8,128)(2,1)} %get-tuple-element.10), calls=%async_computation | async-start | bytes 1048576 | tf_op jit(solution)/shard_map/all_to_all | solution.py:51
  7.6 24.9 %collective-permute-start.4 = (bf16[128,512]{1,0:T(8,128)(2,1)S(1)}, bf16[128,512]{1,0:T(8,128)(2,1)S(1)}, u32[]{:S(2)}, u32[]{:S(2)}) collective-permute-start(bf16[128,512]{1,0:T(8,128)(2,1)S(1)} %get-tuple-element.11), channel_id=1, source_target_pairs={{0,384},{1,129},{2,386},{3,131},{4,388},{5,133},{6,390},{7,135},{8... | collective-permute-start | bytes 393224 | tf_op jit(solution)/shard_map/ppermute | solution.py:46
  24.0 15.3 %collective-permute-start.1 = (bf16[512,512]{1,0:T(8,128)(2,1)S(1)}, bf16[512,512]{1,0:T(8,128)(2,1)S(1)}, u32[]{:S(2)}, u32[]{:S(2)}) collective-permute-start(bf16[512,512]{1,0:T(8,128)(2,1)S(1)} %bitcast.60), channel_id=1, source_target_pairs={{0,480},{8,488},{16,496},{24,504},{32,0},{40,8},{48,16},{56,24},{6... | collective-permute-start | bytes 1572872 | tf_op jit(solution)/shard_map/ppermute | solution.py:33
  28.5 15.9 %collective-permute-start = (bf16[512,512]{1,0:T(8,128)(2,1)S(1)}, bf16[512,512]{1,0:T(8,128)(2,1)S(1)}, u32[]{:S(2)}, u32[]{:S(2)}) collective-permute-start(bf16[512,512]{1,0:T(8,128)(2,1)S(1)} %bitcast.61), channel_id=1, source_target_pairs={{0,32},{8,40},{16,48},{24,56},{32,64},{40,72},{48,80},{56,88},{64,... | collective-permute-start | bytes 1572872 | tf_op jit(solution)/shard_map/ppermute | solution.py:33
  33.4 30.7 %all-to-all-start.1 = ((bf16[4,128,512]{2,1,0:T(8,128)(2,1)}), bf16[4,128,512]{2,1,0:T(8,128)(2,1)S(1)}, u32[]{:S(2)}, u32[]{:S(2)}) async-start(bf16[4,128,512]{2,1,0:T(8,128)(2,1)} %broadcast_in_dim.12), calls=%async_computation.1 | async-start | bytes 1048576 | tf_op jit(solution)/shard_map/all_to_all | solution.py:51
  39.2 14.2 %collective-permute-start.3 = (bf16[512,512]{1,0:T(8,128)(2,1)S(1)}, bf16[512,512]{1,0:T(8,128)(2,1)S(1)}, u32[]{:S(2)}, u32[]{:S(2)}) collective-permute-start(bf16[512,512]{1,0:T(8,128)(2,1)S(1)} %collective-permute-done.1), channel_id=1, source_target_pairs={{0,480},{8,488},{16,496},{24,504},{32,0},{40,8},{48,16},{56,24},{6... | collective-permute-start | bytes 1572872 | tf_op jit(solution)/shard_map/ppermute | solution.py:33
  44.4 16.1 %collective-permute-start.2 = (bf16[512,512]{1,0:T(8,128)(2,1)S(1)}, bf16[512,512]{1,0:T(8,128)(2,1)}, u32[]{:S(2)}, u32[]{:S(2)}) collective-permute-start(bf16[512,512]{1,0:T(8,128)(2,1)S(1)} %collective-permute-done), channel_id=1, source_target_pairs={{0,32},{8,40},{16,48},{24,56},{32,64},{40,72},{48,80},{56,88},{64,... | collective-permute-start | bytes 1572872 | tf_op jit(solution)/shard_map/ppermute | solution.py:33
  53.4 14.1 %collective-permute-start.6 = (bf16[512,512]{1,0:T(8,128)(2,1)S(1)}, bf16[512,512]{1,0:T(8,128)(2,1)S(1)}, u32[]{:S(2)}, u32[]{:S(2)}) collective-permute-start(bf16[512,512]{1,0:T(8,128)(2,1)S(1)} %collective-permute-done.3), channel_id=1, source_target_pairs={{0,480},{8,488},{16,496},{24,504},{32,0},{40,8},{48,16},{56,24},{6... | collective-permute-start | bytes 1572872 | tf_op jit(solution)/shard_map/ppermute | solution.py:33
  60.5 14.2 %collective-permute-start.5 = (bf16[512,512]{1,0:T(8,128)(2,1)}, bf16[512,512]{1,0:T(8,128)(2,1)}, u32[]{:S(2)}, u32[]{:S(2)}) collective-permute-start(bf16[512,512]{1,0:T(8,128)(2,1)} %collective-permute-done.2), channel_id=1, source_target_pairs={{0,32},{8,40},{16,48},{24,56},{32,64},{40,72},{48,80},{56,88},{64,... | collective-permute-start | bytes 1572872 | tf_op jit(solution)/shard_map/ppermute | solution.py:33
  65.6 24.5 %copy-start.4 = (f32[4,4]{1,0:T(4,128)S(1)}, f32[4,4]{1,0:T(4,128)}, u32[]{:S(2)}) copy-start(f32[4,4]{1,0:T(4,128)} %param.16) | copy-start | bytes 196
  65.6 24.6 %copy-start.3 = (bf16[4,256]{1,0:T(4,128)(2,1)S(1)}, bf16[4,256]{1,0:T(4,128)(2,1)}, u32[]{:S(2)}) copy-start(bf16[4,256]{1,0:T(4,128)(2,1)} %param.15) | copy-start | bytes 6148
  69.0 58.2 %copy-start.2 = (f32[256]{0:T(256)S(1)}, f32[256]{0:T(256)}, u32[]{:S(2)}) copy-start(f32[256]{0:T(256)} %param.17) | copy-start | bytes 3076
  79.0 26.4 %all-to-all-start.2 = ((bf16[32,8,384]{2,1,0:T(8,128)(2,1)}), bf16[32,8,384]{2,1,0:T(8,128)(2,1)S(1)}, u32[]{:S(2)}, u32[]{:S(2)}) async-start(bf16[32,8,384]{2,1,0:T(8,128)(2,1)} %bitcast.11), calls=%async_computation.2 | async-start | bytes 393216 | tf_op jit(solution)/shard_map/all_to_all | solution.py:255

commit v2 on v1

--- a/solution.py
+++ b/solution.py
@@ -46,6 +46,12 @@
     return lax.ppermute(x, ("gr", "sp", "tp"), pairs)
 
 
+def moved_along_y(x, by):
+    planes = lax.axis_size("sp") // Y
+    pairs = [(z * Y + y, z * Y + (y + by) % Y) for z in range(planes) for y in range(Y)]
+    return lax.ppermute(x, "sp", pairs)
+
+
 def exchanged_along_y(spread):
     groups = [[z * Y + y for y in range(Y)] for z in range(lax.axis_size("sp") // Y)]
     got = lax.all_to_all(spread, "sp", 0, 0, tiled=True, axis_index_groups=groups)
@@ -59,22 +65,26 @@
     block = exchanged_along_y(spread)
     opposite = from_opposite_plane(own)
     depth = block.shape[0]
-
-    def part(weights, off):
-        first = (mine + (off + planes)) % planes * depth
-        cols = lax.dynamic_slice_in_dim(token_rows, first, depth, 1)
+    row = lax.axis_index("sp").astype(jnp.uint32) % Y
+
+    def part(weights, off, start=0):
+        first = (mine + (off + planes)) % planes * depth + start
+        cols = lax.dynamic_slice_in_dim(token_rows, first, weights.shape[0], 1)
         return jnp.dot(cols, weights, preferred_element_type=F32)
+
+    def far_part(weights, by):
+        return part(weights, far, (row + (Y - by)) % Y * own.shape[0])
 
     total = part(block, 0)
     up = down = block
     for hop in range(1, far):
         down = moved_along_z(down, -1)
         up = moved_along_z(up, 1)
-        if hop + 1 < far:
-            total += part(up, -hop) + part(down, hop)
-    distant = exchanged_along_y(jnp.broadcast_to(opposite[None], (Y, *opposite.shape)))
-    total += part(distant, far)
-    return total + part(up, 1 - far) + part(down, far - 1)
+        beside = moved_along_y(opposite, hop)
+        if hop == 1:
+            total += far_part(opposite, 0)
+        total += far_part(beside, hop) + part(up, -hop) + part(down, hop)
+    return total
 
 
 def in_three(x):
@@ -94,11 +104,16 @@
     return lax.broadcasted_iota(jnp.int32, shape, 0)
 
 
-def spread_kernel(key_ref, value_ref, own_ref, spread_ref):
-    both = jnp.concatenate([key_ref[...], value_ref[...]], axis=1)
-    own_ref[...] = both
-    for y in range(Y):
-        spread_ref[y] = both
+def spread_kernel(key_ref, value_ref, own_ref, spread_ref, sems):
+    cols = key_ref.shape[1]
+    copies = []
+    for ref, cut in ((key_ref, pl.ds(0, cols)), (value_ref, pl.ds(cols, cols))):
+        for to in (own_ref.at[:, cut], *(spread_ref.at[y, :, cut] for y in range(Y))):
+            copies.append(pltpu.make_async_copy(ref, to, sems.at[len(copies)]))
+    for copy in copies:
+        copy.start()
+    for copy in copies:
+        copy.wait()
 
 
 def share_kernel(seqs, sums_ref, cosine_ref, sine_ref, weight_ref, carried_ref, out_ref):
@@ -238,15 +253,16 @@
     cosine, sine, weight, carried = ready
 
     depth = key_weight.shape[0]
-    own, spread = in_vmem(
+    own, spread = pl.pallas_call(
         spread_kernel,
-        [
+        out_shape=[
             jax.ShapeDtypeStruct((depth, 2 * cols), BF16),
             jax.ShapeDtypeStruct((Y, depth, 2 * cols), BF16),
         ],
-        key_weight,
-        value_weight,
-    )
+        in_specs=[pl.BlockSpec(memory_space=pl.ANY)] * 2,
+        out_specs=[pl.BlockSpec(memory_space=pltpu.VMEM)] * 2,
+        scratch_shapes=[pltpu.SemaphoreType.DMA((2 * (Y + 1),))],
+    )(key_weight, value_weight)
     sums = projected(tokens.reshape(seqs * span, width), own, spread)
     whole = jax.ShapeDtypeStruct((cols, lanes + EXTRA), BF16)
 
@@ -260,11 +276,13 @@
     finished = in_vmem(
         functools.partial(owner_kernel, devices, seqs), whole, exchanged(sent), lines, value_rows
     )
+    gathered = exchanged(finished)
+    gain = jnp.broadcast_to(norm_gain[None], (8, cols))
     state, first_read = in_vmem(
         functools.partial(read_kernel, seqs),
         [jax.ShapeDtypeStruct((cols, lanes), F32), jax.ShapeDtypeStruct((seqs, cols), BF16)],
-        exchanged(finished),
-        norm_gain.reshape(1, cols),
+        gathered,
+        gain,
     )
     state_cache = jnp.transpose(state.reshape(heads, HEAD_DIM, lanes), (2, 0, 1))
     return (state_cache, first_read)

time: 130 us -> 142 us (1.092)
  the two profiles are of different devices: /device:TPU:4 before, /device:TPU:6 now
where the time goes in v2:
time: 142 us; the launch traced here: 141 us
  starting transfers between devices  53 us (37%)
  waiting for transfers between devices  45.9 us (32%)
  blocking collectives  21 us (15%)
  matrix products  7.09 us (5%)
  Pallas kernels  6.7 us (5%)
  other arithmetic  3.57 us (3%)
  local copies, waits for them, and re-layouts  2.7 us (2%)
    ppermute x6, waiting for transfers between devices, moved_along_z(): return lax.ppermute(x, ('gr', 'sp'), pairs)  28.1 us
    ppermute x6, starting transfers between devices, moved_along_z(): return lax.ppermute(x, ('gr', 'sp'), pairs)  21.1 us
    all_to_all x1, blocking collectives, exchanged(): return lax.all_to_all(cut, 'sp', 0, 0, tiled=True).reshape(x.shape)  21 us
    all_to_all x1, waiting for transfers between devices, exchanged(): return lax.all_to_all(cut, 'sp', 0, 0, tiled=True).reshape(x.shape)  14.4 us
    ppermute x1, starting transfers between devices, from_opposite_plane(): return lax.ppermute(x, ('gr', 'sp', 'tp'), pairs)  12.7 us
    ppermute x3, starting transfers between devices, moved_along_y(): return lax.ppermute(x, 'sp', pairs)  10.7 us
    dot_general x11, matrix products, part(): return jnp.dot(cols, weights, preferred_element_type=F32)  7.09 us
    pallas_call x3, Pallas kernels, in_vmem(): pl.pallas_call(kernel, out_shape=shapes, in_specs=[space] * len(operands)...  4.62 us
  transfers between devices with their start and end apart: 12, of which 5 were waited for; matrix products, arithmetic and copies ran while one was open for 9% of the time, Pallas kernels for 0%

profile of v2, /device:TPU:6, one launch (start us, length us, event | category | flops | bytes accessed | tf_op | source)
XLA Modules:
  0.0 141.0 jit_solution(16787668333016061186)
XLA Ops:
  0.6 2.1 %shard_map.104 = (bf16[128,512]{1,0:T(8,128)(2,1)}, bf16[4,128,512]{2,1,0:T(8,128)(2,1)}) custom-call(bf16[128,256]{1,0:T(8,128)(2,1)} %key_ref.1, bf16[128,256]{1,0:T(8,128)(2,1)} %value_ref.1), custom_call_target="tpu_custom_call" | custom-call | tf_op jit(solution)/shard_map/pallas_call | solution.py:256
  2.7 4.5 %all-to-all-start = ((bf16[4,128,512]{2,1,0:T(8,128)(2,1)}), bf16[4,128,512]{2,1,0:T(8,128)(2,1)S(1)}, u32[]{:S(2)}, u32[]{:S(2)}) async-start(bf16[4,128,512]{2,1,0:T(8,128)(2,1)} %get-tuple-element.10), calls=%async_computation | async-start | bytes 1048576 | tf_op jit(solution)/shard_map/all_to_all | solution.py:57
  7.2 12.7 %collective-permute-start = (bf16[128,512]{1,0:T(8,128)(2,1)}, bf16[128,512]{1,0:T(8,128)(2,1)S(1)}, u32[]{:S(2)}, u32[]{:S(2)}) collective-permute-start(bf16[128,512]{1,0:T(8,128)(2,1)} %get-tuple-element.11), channel_id=1, source_target_pairs={{0,384},{1,129},{2,386},{3,131},{4,388},{5,133},{6,390},{7,135},{8... | collective-permute-start | bytes 393224 | tf_op jit(solution)/shard_map/ppermute | solution.py:46
  19.9 0.8 reduce_sum.11
  20.7 2.3 %reduce_window_sum.13 = f32[4,4,128]{2,1,0:T(4,128)S(1)} reduce-window(f32[4,4,128]{2,1,0:T(4,128)} %param.12, f32[]{:T(128)} %constant.137.clone.1), window={size=1x1x128 pad=0_0x0_0x127_0}, to_apply=%region_1.0 | reduce-window | flops 260096 | bytes 16388 | tf_op jit(solution)/shard_map/jit(cumsum)/reduce_window_sum | solution.py:233
  23.0 0.1 copy.17
  23.1 0.1 broadcast_in_dim.12
  23.2 0.1 fusion.26
  23.4 0.1 fusion.25
  23.5 3.4 %collective-permute-done = bf16[128,512]{1,0:T(8,128)(2,1)S(1)} collective-permute-done((bf16[128,512]{1,0:T(8,128)(2,1)}, bf16[128,512]{1,0:T(8,128)(2,1)S(1)}, u32[]{:S(2)}, u32[]{:S(2)}) %collective-permute-start) | collective-permute-done | bytes 131104 | tf_op jit(solution)/shard_map/ppermute | solution.py:46
  26.9 5.1 %collective-permute-start.7 = (bf16[128,512]{1,0:T(8,128)(2,1)S(1)}, bf16[128,512]{1,0:T(8,128)(2,1)S(1)}, u32[]{:S(2)}, u32[]{:S(2)}) collective-permute-start(bf16[128,512]{1,0:T(8,128)(2,1)S(1)} %collective-permute-done), channel_id=1, source_target_pairs={{0,24},{8,0},{16,8},{24,16},{32,56},{40,32},{48,40},{56,48},{64,88... | collective-permute-start | bytes 393224 | tf_op jit(solution)/shard_map/ppermute | solution.py:52
  32.2 0.1 copy.16
  32.4 0.1 copy.19.cosine_ref
  32.5 0.1 copy.20.sine_ref
  32.6 0.8 reshape.160
  33.4 0.8 reshape.162
  34.2 2.8 %collective-permute-start.4 = (bf16[128,512]{1,0:T(8,128)(2,1)S(1)}, bf16[128,512]{1,0:T(8,128)(2,1)S(1)}, u32[]{:S(2)}, u32[]{:S(2)}) collective-permute-start(bf16[128,512]{1,0:T(8,128)(2,1)S(1)} %collective-permute-done), channel_id=1, source_target_pairs={{0,16},{8,24},{16,0},{24,8},{32,48},{40,56},{48,32},{56,40},{64,80... | collective-permute-start | bytes 393224 | tf_op jit(solution)/shard_map/ppermute | solution.py:52
  36.9 2.8 %collective-permute-start.1 = (bf16[128,512]{1,0:T(8,128)(2,1)S(1)}, bf16[128,512]{1,0:T(8,128)(2,1)S(1)}, u32[]{:S(2)}, u32[]{:S(2)}) collective-permute-start(bf16[128,512]{1,0:T(8,128)(2,1)S(1)} %collective-permute-done), channel_id=1, source_target_pairs={{0,8},{8,16},{16,24},{24,0},{32,40},{40,48},{48,56},{56,32},{64,72... | collective-permute-start | bytes 393224 | tf_op jit(solution)/shard_map/ppermute | solution.py:52
  39.7 0.0 collective-permute-done.7
  39.7 1.2 fusion.17
  40.9 0.0 all-to-all-done
  40.9 0.0 copy-start
  40.9 3.2 %collective-permute-start.3 = (bf16[512,512]{1,0:T(8,128)(2,1)S(1)}, bf16[512,512]{1,0:T(8,128)(2,1)S(1)}, u32[]{:S(2)}, u32[]{:S(2)}) collective-permute-start(bf16[512,512]{1,0:T(8,128)(2,1)S(1)} %bitcast.63), channel_id=1, source_target_pairs={{0,480},{8,488},{16,496},{24,504},{32,0},{40,8},{48,16},{56,24},{6... | collective-permute-start | bytes 1572872 | tf_op jit(solution)/shard_map/ppermute | solution.py:33
  44.1 2.9 %collective-permute-start.2 = (bf16[512,512]{1,0:T(8,128)(2,1)S(1)}, bf16[512,512]{1,0:T(8,128)(2,1)S(1)}, u32[]{:S(2)}, u32[]{:S(2)}) collective-permute-start(bf16[512,512]{1,0:T(8,128)(2,1)S(1)} %bitcast.64), channel_id=1, source_target_pairs={{0,32},{8,40},{16,48},{24,56},{32,64},{40,72},{48,80},{56,88},{64,... | collective-permute-start | bytes 1572872 | tf_op jit(solution)/shard_map/ppermute | solution.py:33
  47.1 1.5 %fusion.15 = f32[512,512]{1,0:T(8,128)S(1)} fusion(bf16[512,512]{1,0:T(8,128)(2,1)S(1)} %bitcast.65, bf16[512,4096]{1,0:T(8,128)(2,1)} %bitcast.53, u32[]{:T(128)S(6)} %mul.157), kind=kOutput, calls=%fused_computation.20 | convolution fusion | flops 268435456 | bytes 2097156 | tf_op jit(solution)/shard_map/dot_general | solution.py:73
  48.6 1.2 convolution_add_fusion.4
  49.7 6.7 %collective-permute-done.3 = bf16[512,512]{1,0:T(8,128)(2,1)S(1)} collective-permute-done((bf16[512,512]{1,0:T(8,128)(2,1)S(1)}, bf16[512,512]{1,0:T(8,128)(2,1)S(1)}, u32[]{:S(2)}, u32[]{:S(2)}) %collective-permute-start.3) | collective-permute-done | bytes 524320 | tf_op jit(solution)/shard_map/ppermute | solution.py:33
  56.4 5.6 %collective-permute-start.6 = (bf16[512,512]{1,0:T(8,128)(2,1)S(1)}, bf16[512,512]{1,0:T(8,128)(2,1)S(1)}, u32[]{:S(2)}, u32[]{:S(2)}) collective-permute-start(bf16[512,512]{1,0:T(8,128)(2,1)S(1)} %collective-permute-done.3), channel_id=1, source_target_pairs={{0,480},{8,488},{16,496},{24,504},{32,0},{40,8},{48,16},{56,24},{6... | collective-permute-start | bytes 1572872 | tf_op jit(solution)/shard_map/ppermute | solution.py:33
  62.0 0.0 collective-permute-done.2
  62.0 1.9 %collective-permute-start.5 = (bf16[512,512]{1,0:T(8,128)(2,1)S(1)}, bf16[512,512]{1,0:T(8,128)(2,1)S(1)}, u32[]{:S(2)}, u32[]{:S(2)}) collective-permute-start(bf16[512,512]{1,0:T(8,128)(2,1)S(1)} %collective-permute-done.2), channel_id=1, source_target_pairs={{0,32},{8,40},{16,48},{24,56},{32,64},{40,72},{48,80},{56,88},{64,... | collective-permute-start | bytes 1572872 | tf_op jit(solution)/shard_map/ppermute | solution.py:33
  63.9 0.0 copy-done
  63.9 0.4 fusion.11
  64.4 0.4 fusion.13
  64.8 8.6 %collective-permute-done.6 = bf16[512,512]{1,0:T(8,128)(2,1)S(1)} collective-permute-done((bf16[512,512]{1,0:T(8,128)(2,1)S(1)}, bf16[512,512]{1,0:T(8,128)(2,1)S(1)}, u32[]{:S(2)}, u32[]{:S(2)}) %collective-permute-start.6) | collective-permute-done | bytes 524320 | tf_op jit(solution)/shard_map/ppermute | solution.py:33
  73.4 5.6 %collective-permute-start.9 = (bf16[512,512]{1,0:T(8,128)(2,1)S(1)}, bf16[512,512]{1,0:T(8,128)(2,1)S(1)}, u32[]{:S(2)}, u32[]{:S(2)}) collective-permute-start(bf16[512,512]{1,0:T(8,128)(2,1)S(1)} %collective-permute-done.6), channel_id=1, source_target_pairs={{0,480},{8,488},{16,496},{24,504},{32,0},{40,8},{48,16},{56,24},{6... | collective-permute-start | bytes 1572872 | tf_op jit(solution)/shard_map/ppermute | solution.py:33
  79.0 0.4 fusion.7
  79.4 0.0 collective-permute-done.5
  79.4 1.9 %collective-permute-start.8 = (bf16[512,512]{1,0:T(8,128)(2,1)S(1)}, bf16[512,512]{1,0:T(8,128)(2,1)S(1)}, u32[]{:S(2)}, u32[]{:S(2)}) collective-permute-start(bf16[512,512]{1,0:T(8,128)(2,1)S(1)} %collective-permute-done.5), channel_id=1, source_target_pairs={{0,32},{8,40},{16,48},{24,56},{32,64},{40,72},{48,80},{56,88},{64,... | collective-permute-start | bytes 1572872 | tf_op jit(solution)/shard_map/ppermute | solution.py:33
  81.4 0.4 fusion.9
  81.8 0.0 collective-permute-done.4
  81.8 0.3 fusion.4
  82.1 0.0 collective-permute-done.1
  82.1 0.3 fusion.3
  82.4 0.0 copy-start.2
  82.5 0.0 copy-start.1
  82.5 12.8 %collective-permute-done.8 = bf16[512,512]{1,0:T(8,128)(2,1)S(1)} collective-permute-done((bf16[512,512]{1,0:T(8,128)(2,1)S(1)}, bf16[512,512]{1,0:T(8,128)(2,1)S(1)}, u32[]{:S(2)}, u32[]{:S(2)}) %collective-permute-start.8) | collective-permute-done | bytes 524320 | tf_op jit(solution)/shard_map/ppermute | solution.py:33
  95.3 0.4 convolution_add_fusion.1
  95.7 0.0 copy-start.3
  95.8 0.0 collective-permute-done.9
  95.8 0.4 fusion.sums_ref
  96.2 2.7 %shard_map.105 = bf16[256,384]{1,0:T(8,128)(2,1)} custom-call(f32[512,512]{1,0:T(8,128)S(1)} %fusion.sums_ref, f32[128,256]{1,0:T(8,128)S(1)} %copy.19.cosine_ref, f32[128,256]{1,0:T(8,128)S(1)} %copy.20.sine_ref, f32[512,4]{1,0:T(8,128)S(1)} %bitcast.48, bf16[256,128]{1,0:T(8,128)(2,1)S(1)} %pad_bitcast_fusion.carried_ref), custom_call_target="tpu_custom_call" | custom-call | tf_op jit(solution)/shard_map/pallas_call | solution.py:198
  98.9 4.0 %all-to-all-start.1 = ((bf16[32,8,384]{2,1,0:T(8,128)(2,1)}), bf16[32,8,384]{2,1,0:T(8,128)(2,1)S(1)}, u32[]{:S(2)}, u32[]{:S(2)}) async-start(bf16[32,8,384]{2,1,0:T(8,128)(2,1)} %bitcast.10), calls=%async_computation.1 | async-start | bytes 393216 | tf_op jit(solution)/shard_map/all_to_all | solution.py:271
  103.0 0.1 multiply_subtract_fusion
  103.0 0.1 fusion.24
  103.1 0.1 stack_reshape.10
  103.2 0.1 stack_reshape.11
  103.3 0.1 broadcast_in_dim.29
  103.4 0.1 stack_reshape.9
  103.5 0.1 constant_dynamic-slice_fusion
  103.6 0.1 copy.24.values_ref
  103.7 14.4 %all-to-all-done.1 = bf16[32,8,384]{2,1,0:T(8,128)(2,1)S(1)} async-done(((bf16[32,8,384]{2,1,0:T(8,128)(2,1)}), bf16[32,8,384]{2,1,0:T(8,128)(2,1)S(1)}, u32[]{:S(2)}, u32[]{:S(2)}) %all-to-all-start.1) | async-done | bytes 196640 | tf_op jit(solution)/shard_map/all_to_all | solution.py:271
  118.1 0.6 shard_map.106
  118.7 21.0 %all_to_all.15 = bf16[32,8,384]{2,1,0:T(8,128)(2,1)S(1)} all-to-all(bf16[32,8,384]{2,1,0:T(8,128)(2,1)S(1)} %bitcast.51), channel_id=1, replica_groups=mesh['gr'=2,'sp'=32,'tp'=8] {'sp'}, dimensions={0} | all-to-all | bytes 393216 | tf_op jit(solution)/shard_map/all_to_all | solution.py:271
  139.7 1.3 shard_map.107
  (22 shorter events, 0.3 us)
Async XLA Ops:
  2.7 38.2 %all-to-all-start = ((bf16[4,128,512]{2,1,0:T(8,128)(2,1)}), bf16[4,128,512]{2,1,0:T(8,128)(2,1)S(1)}, u32[]{:S(2)}, u32[]{:S(2)}) async-start(bf16[4,128,512]{2,1,0:T(8,128)(2,1)} %get-tuple-element.10), calls=%async_computation | async-start | bytes 1048576 | tf_op jit(solution)/shard_map/all_to_all | solution.py:57
  7.2 19.8 %collective-permute-start = (bf16[128,512]{1,0:T(8,128)(2,1)}, bf16[128,512]{1,0:T(8,128)(2,1)S(1)}, u32[]{:S(2)}, u32[]{:S(2)}) collective-permute-start(bf16[128,512]{1,0:T(8,128)(2,1)} %get-tuple-element.11), channel_id=1, source_target_pairs={{0,384},{1,129},{2,386},{3,131},{4,388},{5,133},{6,390},{7,135},{8... | collective-permute-start | bytes 393224 | tf_op jit(solution)/shard_map/ppermute | solution.py:46
  26.9 12.8 %collective-permute-start.7 = (bf16[128,512]{1,0:T(8,128)(2,1)S(1)}, bf16[128,512]{1,0:T(8,128)(2,1)S(1)}, u32[]{:S(2)}, u32[]{:S(2)}) collective-permute-start(bf16[128,512]{1,0:T(8,128)(2,1)S(1)} %collective-permute-done), channel_id=1, source_target_pairs={{0,24},{8,0},{16,8},{24,16},{32,56},{40,32},{48,40},{56,48},{64,88... | collective-permute-start | bytes 393224 | tf_op jit(solution)/shard_map/ppermute | solution.py:52
  34.2 47.6 %collective-permute-start.4 = (bf16[128,512]{1,0:T(8,128)(2,1)S(1)}, bf16[128,512]{1,0:T(8,128)(2,1)S(1)}, u32[]{:S(2)}, u32[]{:S(2)}) collective-permute-start(bf16[128,512]{1,0:T(8,128)(2,1)S(1)} %collective-permute-done), channel_id=1, source_target_pairs={{0,16},{8,24},{16,0},{24,8},{32,48},{40,56},{48,32},{56,40},{64,80... | collective-permute-start | bytes 393224 | tf_op jit(solution)/shard_map/ppermute | solution.py:52
  36.9 45.2 %collective-permute-start.1 = (bf16[128,512]{1,0:T(8,128)(2,1)S(1)}, bf16[128,512]{1,0:T(8,128)(2,1)S(1)}, u32[]{:S(2)}, u32[]{:S(2)}) collective-permute-start(bf16[128,512]{1,0:T(8,128)(2,1)S(1)} %collective-permute-done), channel_id=1, source_target_pairs={{0,8},{8,16},{16,24},{24,0},{32,40},{40,48},{48,56},{56,32},{64,72... | collective-permute-start | bytes 393224 | tf_op jit(solution)/shard_map/ppermute | solution.py:52
  40.9 23.0 %copy-start = (bf16[4,128,4096]{2,1,0:T(8,128)(2,1)S(1)}, bf16[4,128,4096]{2,1,0:T(8,128)(2,1)}, u32[]{:S(2)}) copy-start(bf16[4,128,4096]{2,1,0:T(8,128)(2,1)} %param.9) | copy-start | bytes 12582916
  40.9 15.5 %collective-permute-start.3 = (bf16[512,512]{1,0:T(8,128)(2,1)S(1)}, bf16[512,512]{1,0:T(8,128)(2,1)S(1)}, u32[]{:S(2)}, u32[]{:S(2)}) collective-permute-start(bf16[512,512]{1,0:T(8,128)(2,1)S(1)} %bitcast.63), channel_id=1, source_target_pairs={{0,480},{8,488},{16,496},{24,504},{32,0},{40,8},{48,16},{56,24},{6... | collective-permute-start | bytes 1572872 | tf_op jit(solution)/shard_map/ppermute | solution.py:33
  44.1 17.9 %collective-permute-start.2 = (bf16[512,512]{1,0:T(8,128)(2,1)S(1)}, bf16[512,512]{1,0:T(8,128)(2,1)S(1)}, u32[]{:S(2)}, u32[]{:S(2)}) collective-permute-start(bf16[512,512]{1,0:T(8,128)(2,1)S(1)} %bitcast.64), channel_id=1, source_target_pairs={{0,32},{8,40},{16,48},{24,56},{32,64},{40,72},{48,80},{56,88},{64,... | collective-permute-start | bytes 1572872 | tf_op jit(solution)/shard_map/ppermute | solution.py:33
  56.4 17.0 %collective-permute-start.6 = (bf16[512,512]{1,0:T(8,128)(2,1)S(1)}, bf16[512,512]{1,0:T(8,128)(2,1)S(1)}, u32[]{:S(2)}, u32[]{:S(2)}) collective-permute-start(bf16[512,512]{1,0:T(8,128)(2,1)S(1)} %collective-permute-done.3), channel_id=1, source_target_pairs={{0,480},{8,488},{16,496},{24,504},{32,0},{40,8},{48,16},{56,24},{6... | collective-permute-start | bytes 1572872 | tf_op jit(solution)/shard_map/ppermute | solution.py:33
  62.0 17.4 %collective-permute-start.5 = (bf16[512,512]{1,0:T(8,128)(2,1)S(1)}, bf16[512,512]{1,0:T(8,128)(2,1)S(1)}, u32[]{:S(2)}, u32[]{:S(2)}) collective-permute-start(bf16[512,512]{1,0:T(8,128)(2,1)S(1)} %collective-permute-done.2), channel_id=1, source_target_pairs={{0,32},{8,40},{16,48},{24,56},{32,64},{40,72},{48,80},{56,88},{64,... | collective-permute-start | bytes 1572872 | tf_op jit(solution)/shard_map/ppermute | solution.py:33
  73.4 22.4 %collective-permute-start.9 = (bf16[512,512]{1,0:T(8,128)(2,1)S(1)}, bf16[512,512]{1,0:T(8,128)(2,1)S(1)}, u32[]{:S(2)}, u32[]{:S(2)}) collective-permute-start(bf16[512,512]{1,0:T(8,128)(2,1)S(1)} %collective-permute-done.6), channel_id=1, source_target_pairs={{0,480},{8,488},{16,496},{24,504},{32,0},{40,8},{48,16},{56,24},{6... | collective-permute-start | bytes 1572872 | tf_op jit(solution)/shard_map/ppermute | solution.py:33
  79.4 15.9 %collective-permute-start.8 = (bf16[512,512]{1,0:T(8,128)(2,1)S(1)}, bf16[512,512]{1,0:T(8,128)(2,1)S(1)}, u32[]{:S(2)}, u32[]{:S(2)}) collective-permute-start(bf16[512,512]{1,0:T(8,128)(2,1)S(1)} %collective-permute-done.5), channel_id=1, source_target_pairs={{0,32},{8,40},{16,48},{24,56},{32,64},{40,72},{48,80},{56,88},{64,... | collective-permute-start | bytes 1572872 | tf_op jit(solution)/shard_map/ppermute | solution.py:33
  82.4 20.9 %copy-start.2 = (f32[4,4]{1,0:T(4,128)S(1)}, f32[4,4]{1,0:T(4,128)}, u32[]{:S(2)}) copy-start(f32[4,4]{1,0:T(4,128)} %param.16) | copy-start | bytes 196
  82.5 21.0 %copy-start.1 = (bf16[4,256]{1,0:T(4,128)(2,1)S(1)}, bf16[4,256]{1,0:T(4,128)(2,1)}, u32[]{:S(2)}) copy-start(bf16[4,256]{1,0:T(4,128)(2,1)} %param.15) | copy-start | bytes 6148
  95.7 44.0 %copy-start.3 = (f32[256]{0:T(256)S(1)}, f32[256]{0:T(256)}, u32[]{:S(2)}) copy-start(f32[256]{0:T(256)} %param.17) | copy-start | bytes 3076
  98.9 19.2 %all-to-all-start.1 = ((bf16[32,8,384]{2,1,0:T(8,128)(2,1)}), bf16[32,8,384]{2,1,0:T(8,128)(2,1)S(1)}, u32[]{:S(2)}, u32[]{:S(2)}) async-start(bf16[32,8,384]{2,1,0:T(8,128)(2,1)} %bitcast.10), calls=%async_computation.1 | async-start | bytes 393216 | tf_op jit(solution)/shard_map/all_to_all | solution.py:271

commit v3 on v2

--- a/solution.py
+++ b/solution.py
@@ -249,8 +249,8 @@
     lines = lax.dynamic_index_in_dim(lines, mine // (devices // heads), 0, keepdims=False)
     value_cols = jnp.repeat(new_value.astype(F32).T, HEAD_DIM, axis=1)
     value_rows = lax.dynamic_slice_in_dim(value_cols, mine * rows, rows, 0)
-    ready = lax.optimization_barrier((cosine, sine, weight, carried))
-    cosine, sine, weight, carried = ready
+    ready = lax.optimization_barrier((cosine, sine, weight, carried, lines, value_rows))
+    cosine, sine, weight, carried, lines, value_rows = ready
 
     depth = key_weight.shape[0]
     own, spread = pl.pallas_call(
@@ -276,13 +276,11 @@
     finished = in_vmem(
         functools.partial(owner_kernel, devices, seqs), whole, exchanged(sent), lines, value_rows
     )
-    gathered = exchanged(finished)
-    gain = jnp.broadcast_to(norm_gain[None], (8, cols))
     state, first_read = in_vmem(
         functools.partial(read_kernel, seqs),
         [jax.ShapeDtypeStruct((cols, lanes), F32), jax.ShapeDtypeStruct((seqs, cols), BF16)],
-        gathered,
-        gain,
+        exchanged(finished),
+        norm_gain.reshape(1, cols),
     )
     state_cache = jnp.transpose(state.reshape(heads, HEAD_DIM, lanes), (2, 0, 1))
     return (state_cache, first_read)

time: 142 us -> 134 us (0.944)
  waiting for transfers between devices: 45.9 us -> 24.8 us
  blocking collectives: 21 us -> 36.9 us
  starting transfers between devices: 53 us -> 49.2 us
    all_to_all x1 -> x2, blocking collectives: 21 us -> 36.9 us  [exchanged(): return lax.all_to_all(cut, 'sp', 0, 0, tiled=True).reshape(x.shape)]
    all_to_all x1 -> x0, waiting for transfers between devices: 14.4 us -> none  [exchanged(): return lax.all_to_all(cut, 'sp', 0, 0, tiled=True).reshape(x.shape)]
    all_to_all x1 -> x0, starting transfers between devices: 4.03 us -> none  [exchanged(): return lax.all_to_all(cut, 'sp', 0, 0, tiled=True).reshape(x.shape)]
    ppermute x1, waiting for transfers between devices: 3.42 us -> 0.01 us  [from_opposite_plane(): return lax.ppermute(x, ('gr', 'sp', 'tp'), pairs)]
    ppermute x6, waiting for transfers between devices: 28.1 us -> 24.8 us  [moved_along_z(): return lax.ppermute(x, ('gr', 'sp'), pairs)]
  transfers between devices with their start and end apart: 12 -> 11, of which waited for: 5 -> 3; matrix products, arithmetic and copies ran while one was open for 9% -> 11% of each run, Pallas kernels for 0% -> 0%
where the time goes in v3:
time: 134 us; the launch traced here: 133 us
  starting transfers between devices  49.2 us (37%)
  blocking collectives  36.9 us (28%)
  waiting for transfers between devices  24.8 us (19%)
  matrix products  7.09 us (5%)
  Pallas kernels  6 us (4%)
  other arithmetic  4.26 us (3%)
  local copies, waits for them, and re-layouts  3.38 us (3%)
    all_to_all x2, blocking collectives, exchanged(): return lax.all_to_all(cut, 'sp', 0, 0, tiled=True).reshape(x.shape)  36.9 us
    ppermute x6, waiting for transfers between devices, moved_along_z(): return lax.ppermute(x, ('gr', 'sp'), pairs)  24.8 us
    ppermute x6, starting transfers between devices, moved_along_z(): return lax.ppermute(x, ('gr', 'sp'), pairs)  21.3 us
    ppermute x1, starting transfers between devices, from_opposite_plane(): return lax.ppermute(x, ('gr', 'sp', 'tp'), pairs)  12.7 us
    ppermute x3, starting transfers between devices, moved_along_y(): return lax.ppermute(x, 'sp', pairs)  10.7 us
    dot_general x11, matrix products, part(): return jnp.dot(cols, weights, preferred_element_type=F32)  7.09 us
    all_to_all x1, starting transfers between devices, exchanged_along_y(): lax.all_to_all(spread, 'sp', 0, 0, tiled=True, axis_index_groups=groups)  4.48 us
    pallas_call x3, Pallas kernels, in_vmem(): pl.pallas_call(kernel, out_shape=shapes, in_specs=[space] * len(operands)...  3.94 us
  transfers between devices with their start and end apart: 11, of which 3 were waited for; matrix products, arithmetic and copies ran while one was open for 11% of the time, Pallas kernels for 0%

profile of v3, /device:TPU:6, one launch (start us, length us, event | category | flops | bytes accessed | tf_op | source)
XLA Modules:
  0.0 132.7 jit_solution(659428291139719867)
XLA Ops:
  0.6 2.1 %shard_map.104 = (bf16[128,512]{1,0:T(8,128)(2,1)}, bf16[4,128,512]{2,1,0:T(8,128)(2,1)}) custom-call(bf16[128,256]{1,0:T(8,128)(2,1)} %key_ref.1, bf16[128,256]{1,0:T(8,128)(2,1)} %value_ref.1), custom_call_target="tpu_custom_call" | custom-call | tf_op jit(solution)/shard_map/pallas_call | solution.py:256
  2.7 4.5 %all-to-all-start = ((bf16[4,128,512]{2,1,0:T(8,128)(2,1)}), bf16[4,128,512]{2,1,0:T(8,128)(2,1)S(1)}, u32[]{:S(2)}, u32[]{:S(2)}) async-start(bf16[4,128,512]{2,1,0:T(8,128)(2,1)} %get-tuple-element.12), calls=%async_computation | async-start | bytes 1048576 | tf_op jit(solution)/shard_map/all_to_all | solution.py:57
  7.2 12.7 %collective-permute-start = (bf16[128,512]{1,0:T(8,128)(2,1)}, bf16[128,512]{1,0:T(8,128)(2,1)S(1)}, u32[]{:S(2)}, u32[]{:S(2)}) collective-permute-start(bf16[128,512]{1,0:T(8,128)(2,1)} %get-tuple-element.13), channel_id=1, source_target_pairs={{0,384},{1,129},{2,386},{3,131},{4,388},{5,133},{6,390},{7,135},{8... | collective-permute-start | bytes 393224 | tf_op jit(solution)/shard_map/ppermute | solution.py:46
  20.0 0.1 multiply_sine_fusion.1
  20.0 0.8 reduce_sum.11
  20.8 2.3 %reduce_window_sum.13 = f32[4,4,128]{2,1,0:T(4,128)S(1)} reduce-window(f32[4,4,128]{2,1,0:T(4,128)} %param.12, f32[]{:T(128)} %constant.137.clone.1), window={size=1x1x128 pad=0_0x0_0x127_0}, to_apply=%region_1.0 | reduce-window | flops 260096 | bytes 16388 | tf_op jit(solution)/shard_map/jit(cumsum)/reduce_window_sum | solution.py:233
  23.1 0.8 reshape.163
  23.9 0.8 reshape.165
  24.6 0.7 convert_bitcast_fusion
  25.3 0.1 copy.17
  25.5 0.1 broadcast_in_dim.20
  25.6 0.1 fusion.26
  25.7 0.1 fusion.25
  25.8 0.1 multiply_subtract_fusion
  25.9 0.1 fusion.24
  26.0 0.1 stack_reshape.10
  26.0 0.1 stack_reshape.11
  26.1 0.7 exp.8
  26.8 0.1 broadcast_in_dim.23
  26.9 0.1 stack_reshape.9
  27.0 0.1 constant_dynamic-slice_fusion
  27.1 0.0 collective-permute-done
  27.1 5.1 %collective-permute-start.7 = (bf16[128,512]{1,0:T(8,128)(2,1)S(1)}, bf16[128,512]{1,0:T(8,128)(2,1)S(1)}, u32[]{:S(2)}, u32[]{:S(2)}) collective-permute-start(bf16[128,512]{1,0:T(8,128)(2,1)S(1)} %collective-permute-done), channel_id=1, source_target_pairs={{0,24},{8,0},{16,8},{24,16},{32,56},{40,32},{48,40},{56,48},{64,88... | collective-permute-start | bytes 393224 | tf_op jit(solution)/shard_map/ppermute | solution.py:52
  32.3 0.1 copy.24.values_ref
  32.4 0.1 copy.16
  32.7 0.1 copy.22.cosine_ref
  32.8 0.1 copy.23.sine_ref
  32.9 2.8 %collective-permute-start.4 = (bf16[128,512]{1,0:T(8,128)(2,1)S(1)}, bf16[128,512]{1,0:T(8,128)(2,1)S(1)}, u32[]{:S(2)}, u32[]{:S(2)}) collective-permute-start(bf16[128,512]{1,0:T(8,128)(2,1)S(1)} %collective-permute-done), channel_id=1, source_target_pairs={{0,16},{8,24},{16,0},{24,8},{32,48},{40,56},{48,32},{56,40},{64,80... | collective-permute-start | bytes 393224 | tf_op jit(solution)/shard_map/ppermute | solution.py:52
  35.6 2.8 %collective-permute-start.1 = (bf16[128,512]{1,0:T(8,128)(2,1)S(1)}, bf16[128,512]{1,0:T(8,128)(2,1)S(1)}, u32[]{:S(2)}, u32[]{:S(2)}) collective-permute-start(bf16[128,512]{1,0:T(8,128)(2,1)S(1)} %collective-permute-done), channel_id=1, source_target_pairs={{0,8},{8,16},{16,24},{24,0},{32,40},{40,48},{48,56},{56,32},{64,72... | collective-permute-start | bytes 393224 | tf_op jit(solution)/shard_map/ppermute | solution.py:52
  38.4 0.0 collective-permute-done.7
  38.4 1.2 fusion.17
  39.6 0.0 all-to-all-done
  39.6 0.0 copy-start.1
  39.6 4.4 %collective-permute-start.3 = (bf16[512,512]{1,0:T(8,128)(2,1)S(1)}, bf16[512,512]{1,0:T(8,128)(2,1)S(1)}, u32[]{:S(2)}, u32[]{:S(2)}) collective-permute-start(bf16[512,512]{1,0:T(8,128)(2,1)S(1)} %bitcast.66), channel_id=1, source_target_pairs={{0,480},{8,488},{16,496},{24,504},{32,0},{40,8},{48,16},{56,24},{6... | collective-permute-start | bytes 1572872 | tf_op jit(solution)/shard_map/ppermute | solution.py:33
  44.0 1.9 %collective-permute-start.2 = (bf16[512,512]{1,0:T(8,128)(2,1)S(1)}, bf16[512,512]{1,0:T(8,128)(2,1)S(1)}, u32[]{:S(2)}, u32[]{:S(2)}) collective-permute-start(bf16[512,512]{1,0:T(8,128)(2,1)S(1)} %bitcast.67), channel_id=1, source_target_pairs={{0,32},{8,40},{16,48},{24,56},{32,64},{40,72},{48,80},{56,88},{64,... | collective-permute-start | bytes 1572872 | tf_op jit(solution)/shard_map/ppermute | solution.py:33
  46.0 1.5 %fusion.15 = f32[512,512]{1,0:T(8,128)S(1)} fusion(bf16[512,512]{1,0:T(8,128)(2,1)S(1)} %bitcast.68, bf16[512,4096]{1,0:T(8,128)(2,1)} %bitcast.56, u32[]{:T(128)S(6)} %mul.157), kind=kOutput, calls=%fused_computation.20 | convolution fusion | flops 268435456 | bytes 2097156 | tf_op jit(solution)/shard_map/dot_general | solution.py:73
  47.4 1.2 convolution_add_fusion.4
  48.6 6.2 %collective-permute-done.3 = bf16[512,512]{1,0:T(8,128)(2,1)S(1)} collective-permute-done((bf16[512,512]{1,0:T(8,128)(2,1)S(1)}, bf16[512,512]{1,0:T(8,128)(2,1)S(1)}, u32[]{:S(2)}, u32[]{:S(2)}) %collective-permute-start.3) | collective-permute-done | bytes 524320 | tf_op jit(solution)/shard_map/ppermute | solution.py:33
  54.9 5.6 %collective-permute-start.6 = (bf16[512,512]{1,0:T(8,128)(2,1)S(1)}, bf16[512,512]{1,0:T(8,128)(2,1)S(1)}, u32[]{:S(2)}, u32[]{:S(2)}) collective-permute-start(bf16[512,512]{1,0:T(8,128)(2,1)S(1)} %collective-permute-done.3), channel_id=1, source_target_pairs={{0,480},{8,488},{16,496},{24,504},{32,0},{40,8},{48,16},{56,24},{6... | collective-permute-start | bytes 1572872 | tf_op jit(solution)/shard_map/ppermute | solution.py:33
  60.4 0.0 collective-permute-done.2
  60.5 1.9 %collective-permute-start.5 = (bf16[512,512]{1,0:T(8,128)(2,1)S(1)}, bf16[512,512]{1,0:T(8,128)(2,1)S(1)}, u32[]{:S(2)}, u32[]{:S(2)}) collective-permute-start(bf16[512,512]{1,0:T(8,128)(2,1)S(1)} %collective-permute-done.2), channel_id=1, source_target_pairs={{0,32},{8,40},{16,48},{24,56},{32,64},{40,72},{48,80},{56,88},{64,... | collective-permute-start | bytes 1572872 | tf_op jit(solution)/shard_map/ppermute | solution.py:33
  62.4 0.0 copy-done.1
  62.4 0.4 fusion.11
  62.8 0.4 fusion.13
  63.3 7.1 %collective-permute-done.6 = bf16[512,512]{1,0:T(8,128)(2,1)S(1)} collective-permute-done((bf16[512,512]{1,0:T(8,128)(2,1)S(1)}, bf16[512,512]{1,0:T(8,128)(2,1)S(1)}, u32[]{:S(2)}, u32[]{:S(2)}) %collective-permute-start.6) | collective-permute-done | bytes 524320 | tf_op jit(solution)/shard_map/ppermute | solution.py:33
  70.4 5.6 %collective-permute-start.9 = (bf16[512,512]{1,0:T(8,128)(2,1)S(1)}, bf16[512,512]{1,0:T(8,128)(2,1)S(1)}, u32[]{:S(2)}, u32[]{:S(2)}) collective-permute-start(bf16[512,512]{1,0:T(8,128)(2,1)S(1)} %collective-permute-done.6), channel_id=1, source_target_pairs={{0,480},{8,488},{16,496},{24,504},{32,0},{40,8},{48,16},{56,24},{6... | collective-permute-start | bytes 1572872 | tf_op jit(solution)/shard_map/ppermute | solution.py:33
  76.0 0.4 fusion.7
  76.5 0.0 collective-permute-done.5
  76.5 1.9 %collective-permute-start.8 = (bf16[512,512]{1,0:T(8,128)(2,1)S(1)}, bf16[512,512]{1,0:T(8,128)(2,1)S(1)}, u32[]{:S(2)}, u32[]{:S(2)}) collective-permute-start(bf16[512,512]{1,0:T(8,128)(2,1)S(1)} %collective-permute-done.5), channel_id=1, source_target_pairs={{0,32},{8,40},{16,48},{24,56},{32,64},{40,72},{48,80},{56,88},{64,... | collective-permute-start | bytes 1572872 | tf_op jit(solution)/shard_map/ppermute | solution.py:33
  78.4 0.4 fusion.9
  78.8 0.0 collective-permute-done.4
  78.8 0.3 fusion.4
  79.1 0.0 collective-permute-done.1
  79.1 0.3 fusion.3
  79.5 11.4 %collective-permute-done.8 = bf16[512,512]{1,0:T(8,128)(2,1)S(1)} collective-permute-done((bf16[512,512]{1,0:T(8,128)(2,1)S(1)}, bf16[512,512]{1,0:T(8,128)(2,1)S(1)}, u32[]{:S(2)}, u32[]{:S(2)}) %collective-permute-start.8) | collective-permute-done | bytes 524320 | tf_op jit(solution)/shard_map/ppermute | solution.py:33
  90.9 0.4 convolution_add_fusion.1
  91.4 0.0 copy-start
  91.4 0.0 collective-permute-done.9
  91.4 0.4 fusion.sums_ref
  91.8 2.0 %shard_map.105 = bf16[256,384]{1,0:T(8,128)(2,1)S(1)} custom-call(f32[512,512]{1,0:T(8,128)S(1)} %fusion.sums_ref, f32[128,256]{1,0:T(8,128)S(1)} %copy.22.cosine_ref, f32[128,256]{1,0:T(8,128)S(1)} %copy.23.sine_ref, f32[512,4]{1,0:T(8,128)S(1)} %bitcast.49, bf16[256,128]{1,0:T(8,128)(2,1)S(1)} %pad_bitcast_fusion.carried_ref), custom_call_target="tpu_custom_call" | custom-call | tf_op jit(solution)/shard_map/pallas_call | solution.py:198
  93.9 18.0 %all_to_all.15 = bf16[32,8,384]{2,1,0:T(8,128)(2,1)S(1)} all-to-all(bf16[32,8,384]{2,1,0:T(8,128)(2,1)S(1)} %bitcast.50), channel_id=1, replica_groups=mesh['gr'=2,'sp'=32,'tp'=8] {'sp'}, dimensions={0} | all-to-all | bytes 393216 | tf_op jit(solution)/shard_map/all_to_all | solution.py:271
  111.8 0.6 shard_map.106
  112.4 18.9 %all_to_all.16 = bf16[32,8,384]{2,1,0:T(8,128)(2,1)S(1)} all-to-all(bf16[32,8,384]{2,1,0:T(8,128)(2,1)S(1)} %bitcast.52), channel_id=1, replica_groups=mesh['gr'=2,'sp'=32,'tp'=8] {'sp'}, dimensions={0} | all-to-all | bytes 393216 | tf_op jit(solution)/shard_map/all_to_all | solution.py:271
  131.4 1.3 shard_map.107
  (16 shorter events, 0.2 us)
Async XLA Ops:
  2.7 36.9 %all-to-all-start = ((bf16[4,128,512]{2,1,0:T(8,128)(2,1)}), bf16[4,128,512]{2,1,0:T(8,128)(2,1)S(1)}, u32[]{:S(2)}, u32[]{:S(2)}) async-start(bf16[4,128,512]{2,1,0:T(8,128)(2,1)} %get-tuple-element.12), calls=%async_computation | async-start | bytes 1048576 | tf_op jit(solution)/shard_map/all_to_all | solution.py:57
  7.2 20.0 %collective-permute-start = (bf16[128,512]{1,0:T(8,128)(2,1)}, bf16[128,512]{1,0:T(8,128)(2,1)S(1)}, u32[]{:S(2)}, u32[]{:S(2)}) collective-permute-start(bf16[128,512]{1,0:T(8,128)(2,1)} %get-tuple-element.13), channel_id=1, source_target_pairs={{0,384},{1,129},{2,386},{3,131},{4,388},{5,133},{6,390},{7,135},{8... | collective-permute-start | bytes 393224 | tf_op jit(solution)/shard_map/ppermute | solution.py:46
  27.1 11.3 %collective-permute-start.7 = (bf16[128,512]{1,0:T(8,128)(2,1)S(1)}, bf16[128,512]{1,0:T(8,128)(2,1)S(1)}, u32[]{:S(2)}, u32[]{:S(2)}) collective-permute-start(bf16[128,512]{1,0:T(8,128)(2,1)S(1)} %collective-permute-done), channel_id=1, source_target_pairs={{0,24},{8,0},{16,8},{24,16},{32,56},{40,32},{48,40},{56,48},{64,88... | collective-permute-start | bytes 393224 | tf_op jit(solution)/shard_map/ppermute | solution.py:52
  32.9 46.0 %collective-permute-start.4 = (bf16[128,512]{1,0:T(8,128)(2,1)S(1)}, bf16[128,512]{1,0:T(8,128)(2,1)S(1)}, u32[]{:S(2)}, u32[]{:S(2)}) collective-permute-start(bf16[128,512]{1,0:T(8,128)(2,1)S(1)} %collective-permute-done), channel_id=1, source_target_pairs={{0,16},{8,24},{16,0},{24,8},{32,48},{40,56},{48,32},{56,40},{64,80... | collective-permute-start | bytes 393224 | tf_op jit(solution)/shard_map/ppermute | solution.py:52
  35.6 43.5 %collective-permute-start.1 = (bf16[128,512]{1,0:T(8,128)(2,1)S(1)}, bf16[128,512]{1,0:T(8,128)(2,1)S(1)}, u32[]{:S(2)}, u32[]{:S(2)}) collective-permute-start(bf16[128,512]{1,0:T(8,128)(2,1)S(1)} %collective-permute-done), channel_id=1, source_target_pairs={{0,8},{8,16},{16,24},{24,0},{32,40},{40,48},{48,56},{56,32},{64,72... | collective-permute-start | bytes 393224 | tf_op jit(solution)/shard_map/ppermute | solution.py:52
  39.6 22.8 %copy-start.1 = (bf16[4,128,4096]{2,1,0:T(8,128)(2,1)S(1)}, bf16[4,128,4096]{2,1,0:T(8,128)(2,1)}, u32[]{:S(2)}) copy-start(bf16[4,128,4096]{2,1,0:T(8,128)(2,1)} %param.9) | copy-start | bytes 12582916
  39.6 15.2 %collective-permute-start.3 = (bf16[512,512]{1,0:T(8,128)(2,1)S(1)}, bf16[512,512]{1,0:T(8,128)(2,1)S(1)}, u32[]{:S(2)}, u32[]{:S(2)}) collective-permute-start(bf16[512,512]{1,0:T(8,128)(2,1)S(1)} %bitcast.66), channel_id=1, source_target_pairs={{0,480},{8,488},{16,496},{24,504},{32,0},{40,8},{48,16},{56,24},{6... | collective-permute-start | bytes 1572872 | tf_op jit(solution)/shard_map/ppermute | solution.py:33
  44.0 16.4 %collective-permute-start.2 = (bf16[512,512]{1,0:T(8,128)(2,1)S(1)}, bf16[512,512]{1,0:T(8,128)(2,1)S(1)}, u32[]{:S(2)}, u32[]{:S(2)}) collective-permute-start(bf16[512,512]{1,0:T(8,128)(2,1)S(1)} %bitcast.67), channel_id=1, source_target_pairs={{0,32},{8,40},{16,48},{24,56},{32,64},{40,72},{48,80},{56,88},{64,... | collective-permute-start | bytes 1572872 | tf_op jit(solution)/shard_map/ppermute | solution.py:33
  54.9 15.6 %collective-permute-start.6 = (bf16[512,512]{1,0:T(8,128)(2,1)S(1)}, bf16[512,512]{1,0:T(8,128)(2,1)S(1)}, u32[]{:S(2)}, u32[]{:S(2)}) collective-permute-start(bf16[512,512]{1,0:T(8,128)(2,1)S(1)} %collective-permute-done.3), channel_id=1, source_target_pairs={{0,480},{8,488},{16,496},{24,504},{32,0},{40,8},{48,16},{56,24},{6... | collective-permute-start | bytes 1572872 | tf_op jit(solution)/shard_map/ppermute | solution.py:33
  60.5 16.0 %collective-permute-start.5 = (bf16[512,512]{1,0:T(8,128)(2,1)S(1)}, bf16[512,512]{1,0:T(8,128)(2,1)S(1)}, u32[]{:S(2)}, u32[]{:S(2)}) collective-permute-start(bf16[512,512]{1,0:T(8,128)(2,1)S(1)} %collective-permute-done.2), channel_id=1, source_target_pairs={{0,32},{8,40},{16,48},{24,56},{32,64},{40,72},{48,80},{56,88},{64,... | collective-permute-start | bytes 1572872 | tf_op jit(solution)/shard_map/ppermute | solution.py:33
  70.4 20.9 %collective-permute-start.9 = (bf16[512,512]{1,0:T(8,128)(2,1)S(1)}, bf16[512,512]{1,0:T(8,128)(2,1)S(1)}, u32[]{:S(2)}, u32[]{:S(2)}) collective-permute-start(bf16[512,512]{1,0:T(8,128)(2,1)S(1)} %collective-permute-done.6), channel_id=1, source_target_pairs={{0,480},{8,488},{16,496},{24,504},{32,0},{40,8},{48,16},{56,24},{6... | collective-permute-start | bytes 1572872 | tf_op jit(solution)/shard_map/ppermute | solution.py:33
  76.5 14.4 %collective-permute-start.8 = (bf16[512,512]{1,0:T(8,128)(2,1)S(1)}, bf16[512,512]{1,0:T(8,128)(2,1)S(1)}, u32[]{:S(2)}, u32[]{:S(2)}) collective-permute-start(bf16[512,512]{1,0:T(8,128)(2,1)S(1)} %collective-permute-done.5), channel_id=1, source_target_pairs={{0,32},{8,40},{16,48},{24,56},{32,64},{40,72},{48,80},{56,88},{64,... | collective-permute-start | bytes 1572872 | tf_op jit(solution)/shard_map/ppermute | solution.py:33
  91.4 40.0 %copy-start = (f32[256]{0:T(256)S(1)}, f32[256]{0:T(256)}, u32[]{:S(2)}) copy-start(f32[256]{0:T(256)} %param.17) | copy-start | bytes 3076
